TPU v7x, 32 devices: a whole 2x2x4 slice. The times are simulated.
32 devices in a mesh: ep: 8 (over z, x), tp: 4 (over y, core).
Axes of the slice: x: 2, y: 2, z: 4, core: 2. Of those that a mesh axis runs over, the one named last changes fastest.
Arguments:
- queries: bfloat16 [2048, 1024], P('ep', 'tp'), may hold values from -6 to 6
- key_rows: bfloat16 [2048, 1024], P('ep', 'tp'), may hold values from -6 to 6
- value_rows: bfloat16 [2048, 1024], P('ep', 'tp'), may hold values from -6 to 6
- out_gate: bfloat16 [2048, 1024], P('ep', 'tp'), may hold values from -6 to 6
- log_decay: float32 [2048, 8], P('ep', 'tp'), may hold values from -3 to 0, as said below
- head_gain: float32 [8, 128], P('tp'), may hold values from 0.1 to 1.9
- out_weight: bfloat16 [1024, 2048], P('tp'), may hold values from -0.1875 to 0.1875
- moe_input: bfloat16 [1024, 2048], P('ep'), may hold values from -6 to 6
- moe_gain: float32 [2048], replicated, may hold values from 0.1 to 1.9
- expert_gate: bfloat16 [8, 2048, 3584], P('ep', None, 'tp'), may hold values from -0.125 to 0.125
- expert_up: bfloat16 [8, 2048, 3584], P('ep', None, 'tp'), may hold values from -0.125 to 0.125
- expert_down: bfloat16 [8, 3584, 2048], P('ep', 'tp'), may hold values from -0.125 to 0.125
- route_ids: int32 [1024, 2], P('ep'), may hold values from 0 to 7, all different within a row; in each aligned block of 128 rows (0 to 127, 128 to 255, ...) at most 64 rows name the same one
- route_weights: float32 [1024, 2], P('ep'), may hold values from 0.2 to 1
Outputs:
- mixer_out: bfloat16 [2048, 2048], P(('ep', 'tp'))
- expert_out: bfloat16 [1024, 2048], P('ep', 'tp')
Inputs may be any that keep to these rules, and one draw needn't show every extreme that they name: `route_ids`: among the 2 entries of a row no expert repeats. In each aligned block of 128 rows (the rows of one index of ep) no expert is named more than 64 times, a bound that some block reaches. `log_decay`: every entry is negative.
All inputs are finite; a program needn't handle non-finite values.
Results may differ from a plain program's by a relative error of at most 0.017.
Values may be sent and summed in bfloat16 or wider, within the bound.
A program may use at most 64 MiB of HBM per device.

v0:
```python
import functools

import jax
import jax.numpy as jnp
from jax import lax
from jax.experimental import pallas as pl
from jax.experimental.pallas import tpu as pltpu
from jax.sharding import PartitionSpec as P

epsilon = 1e-06
CHUNKS = 2
PARTS = 2
BF = jnp.bfloat16
F32 = jnp.float32


def dot(a, b, dims=(((1,), (0,)), ((), ()))):
    return lax.dot_general(a, b, dims, preferred_element_type=F32)


def layer_kernel(
    n, cap, heads,
    q_ref, k_ref, v_ref, g_ref, ld_ref, gain_ref, tok_ref, norm_ref, ids_ref, rw_ref,
    ow_hbm, wg_hbm, wu_hbm, wd_hbm,
    mixer_ref, expert_ref,
    ow, wg, wu, wd, x, part, near, half, far, done, back,
    st, st_in, tot, tot_in, inner, ho, mx, mr1, ms, mr2,
    w_sem, disp_s, disp_r, st_s, st_r, tot_s, tot_r, fwd_s, fwd_r,
    red_s, red_r, redy_s, redy_r, mix_s, mix_r, ret_s, ret_r,
    piece_ref, hi_ref, lo_ref,
):
    i, j = lax.axis_index("ep"), lax.axis_index("tp")
    j1 = j + 1 - 2 * lax.rem(j, 2)
    j2 = lax.rem(j + 2, 4)
    j3 = lax.rem(j1 + 2, 4)
    places = (j, j1, j2, j3)
    rows = n * cap
    step = rows // CHUNKS
    width = x.shape[2]
    dim = gain_ref.shape[1]
    length = q_ref.shape[0]
    quarter = length // 4

    def shift(p):
        return (p + 1) // 2 if p % 2 else n - p // 2

    def ahead(p):
        return lax.rem(i + shift(p), n)

    def behind(p):
        return lax.rem(i + n - shift(p), n)

    def send(src, dst, ss, rs, dev):
        return pltpu.make_async_remote_copy(
            src_ref=src, dst_ref=dst, send_sem=ss, recv_sem=rs, device_id=dev,
            device_id_type=pl.DeviceIdType.MESH,
        )

    loads = [
        pltpu.make_async_copy(a, b, w_sem.at[m])
        for m, (a, b) in enumerate(((ow_hbm, ow), (wg_hbm, wg), (wu_hbm, wu), (wd_hbm, wd)))
    ]
    for c in loads:
        c.start()
    barrier = pltpu.get_barrier_semaphore()
    for d in range(1, n):
        pl.semaphore_signal(barrier, inc=1, device_id=(ahead(d), j), device_id_type=pl.DeviceIdType.MESH)
    for peer in (j1, j2):
        pl.semaphore_signal(barrier, inc=1, device_id=(i, peer), device_id_type=pl.DeviceIdType.MESH)

    tokens, top = ids_ref.shape
    lanes = -(-n // 128) * 128
    rows_f = tok_ref[...].astype(F32)
    scale = lax.rsqrt(jnp.mean(rows_f * rows_f, axis=-1, keepdims=True) + epsilon)
    mine = pl.ds(pl.multiple_of(j * width, width), width)
    normed = (tok_ref[:, mine].astype(F32) * scale * norm_ref[:, mine]).astype(BF)
    expert = lax.broadcasted_iota(jnp.int32, (tokens, lanes), 1)
    named = [ids_ref[:, t : t + 1] == expert for t in range(top)]
    strict = lax.broadcasted_iota(jnp.int32, (tokens, tokens), 0) > lax.broadcasted_iota(
        jnp.int32, (tokens, tokens), 1
    )
    held = sum(jnp.where(m, 1.0, 0.0) for m in named)
    before = dot(jnp.where(strict, 1.0, 0.0).astype(BF), held.astype(BF))
    slot = lax.broadcasted_iota(jnp.int32, (tokens, rows), 1)
    pick, comb = 0.0, 0.0
    for t in range(top):
        rank = jnp.sum(jnp.where(named[t], before, 0.0), axis=1, keepdims=True).astype(jnp.int32)
        d = ids_ref[:, t : t + 1] - i
        d = jnp.where(d < 0, d + n, d)
        place = jnp.where(d == 0, 0, jnp.where(2 * d <= n, 2 * d - 1, 2 * (n - d)))
        hit = slot == place * cap + rank
        pick = pick + jnp.where(hit, 1.0, 0.0)
        comb = comb + jnp.where(hit, rw_ref[:, t : t + 1], 0.0)
    piece = dot(pick.T.astype(BF), normed).astype(BF)
    piece_ref[...] = piece
    x[0, 0:cap, :] = piece[0:cap]
    pl.semaphore_wait(barrier, n + 1)

    sent = []
    disp = [None] * n
    for d in range(1, n):
        r = pl.ds(d * cap, cap)
        disp[d] = send(piece_ref.at[r], x.at[0, r], disp_s.at[d], disp_r.at[d], (ahead(d), j))
        disp[d].start()
        sent.append(disp[d])

    tot[...] = jnp.zeros_like(tot)
    hi = comb.astype(BF)
    hi_ref[...] = hi
    lo_ref[...] = (comb - hi.astype(F32)).astype(BF)
    causal = lax.broadcasted_iota(jnp.int32, (length, length), 0) >= lax.broadcasted_iota(
        jnp.int32, (length, length), 1
    )
    lower = jnp.where(causal, 1.0, 0.0)
    cum = [
        lax.dot_general(
            lower, jnp.broadcast_to(ld_ref[:, h : h + 1], (length, dim)), (((1,), (0,)), ((), ())),
            precision=lax.Precision.HIGHEST, preferred_element_type=F32,
        )
        for h in range(heads)
    ]

    for h in range(heads):
        c = slice(h * dim, (h + 1) * dim)
        total = cum[h][length - 1 : length, :]
        keys = k_ref[:, c].astype(F32) * jnp.exp(total - cum[h])
        st[h * dim : (h + 1) * dim, :] = dot(keys.T.astype(BF), v_ref[:, c]).astype(BF)
        tot[h : h + 1, :] = total
    st_c, tot_c = [None] * n, [None] * n
    for d in range(1, n):
        later = (lax.rem(i + d, n), j)
        st_c[d] = send(st, st_in.at[d], st_s.at[d], st_r.at[d], later)
        tot_c[d] = send(tot, tot_in.at[d], tot_s.at[d], tot_r.at[d], later)

    y_c, c0_c, c2_c = [], [], []
    small = step // PARTS
    group = n // (CHUNKS * PARTS)
    for u in range(CHUNKS * PARTS):
        r = pl.ds(u * small, small)
        y_c.append(send(x.at[0, r], x.at[2, r], fwd_s.at[u, 0], fwd_r.at[u, 0], (i, j2)))
        c0_c.append(send(x.at[0, r], x.at[1, r], fwd_s.at[u, 1], fwd_r.at[u, 1], (i, j1)))
        c2_c.append(send(x.at[2, r], x.at[3, r], fwd_s.at[u, 2], fwd_r.at[u, 2], (i, j1)))
    sent += y_c + c0_c + c2_c

    def forward(u):
        for d in range(max(1, u * group), (u + 1) * group):
            disp[d].wait_recv()
        y_c[u].start()
        c0_c[u].start()

    def relay(u):
        y_c[u].wait_recv()
        c2_c[u].start()

    for u in range(PARTS):
        forward(u)
    for d in range(1, n):
        @pl.when(i + d < n)
        def _():
            st_c[d].start()
            tot_c[d].start()

    for h in range(heads):
        c = slice(h * dim, (h + 1) * dim)
        scores = dot(q_ref[:, c], k_ref[:, c], (((1,), (1,)), ((), ()))) * dim ** (-0.5)
        spread = jnp.where(causal, cum[h][:, 0:1] - cum[h].T[0:1, :], -jnp.inf)
        inner[:, c] = dot((scores * jnp.exp(spread)).astype(BF), v_ref[:, c])

    for u in range(PARTS):
        forward(PARTS + u)
        relay(u)
    loads[0].wait()
    for c in loads[1:]:
        c.wait()

    def stripe(m):
        return pl.ds(pl.multiple_of(places[m] * quarter, quarter), quarter)

    mix_a = send(mx.at[stripe(1)], mr1.at[0], mix_s.at[0], mix_r.at[0], (i, j1))
    mix_b = send(mx.at[stripe(3)], mr1.at[1], mix_s.at[1], mix_r.at[1], (i, j1))
    mix_c = send(ms, mr2, mix_s.at[2], mix_r.at[2], (i, j2))
    sent += [mix_a, mix_b, mix_c]

    def retention():
        entering = jnp.zeros((heads * dim, dim), F32)
        for d in range(n - 1, 0, -1):
            @pl.when(i >= d)
            def _():
                st_c[d].wait_recv()
                tot_c[d].wait_recv()

            @pl.when(i < d)
            def _():
                st_in[d] = jnp.zeros(st_in.shape[1:], BF)
                tot_in[d] = jnp.zeros(tot_in.shape[1:], F32)

            decay = jnp.concatenate(
                [jnp.broadcast_to(jnp.exp(tot_in[d, h : h + 1, :]), (dim, dim)) for h in range(heads)], axis=0
            )
            entering = decay * entering + st_in[d].astype(F32)
        entering = entering.astype(BF)
        for h in range(heads):
            c = slice(h * dim, (h + 1) * dim)
            queries = (q_ref[:, c].astype(F32) * jnp.exp(cum[h])).astype(BF)
            kept = inner[:, c] + dot(queries, entering[h * dim : (h + 1) * dim, :])
            normed = kept * lax.rsqrt(jnp.mean(kept * kept, axis=-1, keepdims=True) + epsilon)
            ho[:, c] = (normed * gain_ref[h : h + 1, :] * jax.nn.silu(g_ref[:, c].astype(F32))).astype(BF)
        mx[...] = dot(ho[...], ow[...]).astype(BF)

        mix_b.start()
        mix_a.start()

    red, red_y = [], []
    for g in range(CHUNKS):
        r = pl.ds(g * step, step)
        red.append((
            send(part.at[1, r], near.at[0, r], red_s.at[g, 0], red_r.at[g, 0], (i, j1)),
            send(part.at[3, r], near.at[1, r], red_s.at[g, 1], red_r.at[g, 1], (i, j1)),
        ))
        sent += list(red[-1])
    for u in range(CHUNKS * PARTS):
        r = pl.ds(u * small, small)
        red_y.append(send(half.at[r], far.at[r], redy_s.at[u], redy_r.at[u], (i, j2)))
    sent += red_y

    def block(m):
        return pl.ds(pl.multiple_of(places[m] * width, width), width)

    def experts(g, between):
        r = pl.ds(g * step, step)
        gate, up = 0.0, 0.0
        for m in (0, 2, 1, 3):
            if m == 1:
                for u in range(g * PARTS, (g + 1) * PARTS):
                    c0_c[u].wait_recv()
                    c2_c[u].wait_recv()
            gate = gate + dot(x[m, r, :], wg[block(m), :])
            up = up + dot(x[m, r, :], wu[block(m), :])
        hidden = (jax.nn.silu(gate) * up).astype(BF)
        between()
        for m in (3, 2, 1, 0):
            part[m, r, :] = dot(hidden, wd[:, block(m)]).astype(BF)
            if m == 3:
                red[g][1].start()
            if m == 1:
                red[g][0].start()
                cross(g)

    def cross(g):
        red[g][1].wait_recv()
        for u in range(g * PARTS, (g + 1) * PARTS):
            r = pl.ds(u * small, small)
            half[r, :] = (part[2, r, :].astype(F32) + near[1, r, :].astype(F32)).astype(BF)
            red_y[u].start()

    ret = [None] * n
    for d in range(n):
        r = pl.ds(d * cap, cap)
        if d:
            ret[d] = send(done.at[r], back.at[r], ret_s.at[d], ret_r.at[d], (behind(d), j))
            sent.append(ret[d])

    def home(g):
        red[g][0].wait_recv()
        for u in range(g * PARTS, (g + 1) * PARTS):
            r = pl.ds(u * small, small)
            red_y[u].wait_recv()
            done[r, :] = (
                part[0, r, :].astype(F32) + near[0, r, :].astype(F32) + far[r, :].astype(F32)
            ).astype(BF)
            for d in range(u * group, (u + 1) * group):
                if d:
                    ret[d].start()
                else:
                    back[pl.ds(0, cap), :] = done[pl.ds(0, cap), :]

    def mix_cross():
        mix_b.wait_recv()
        ms[...] = (mx[stripe(2), :].astype(F32) + mr1[1].astype(F32)).astype(BF)
        mix_c.start()

    experts(0, lambda: None)
    for u in range(PARTS, CHUNKS * PARTS):
        relay(u)
    retention()
    for g in range(1, CHUNKS):
        experts(g, mix_cross if g == 1 else lambda: None)
        home(g - 1)
    mix_a.wait_recv()
    mix_c.wait_recv()
    mixer_ref[...] = (
        mx[stripe(0), :].astype(F32) + mr1[0].astype(F32) + mr2[...].astype(F32)
    ).astype(BF)
    home(CHUNKS - 1)
    for d in range(1, n):
        ret[d].wait_recv()
    expert_ref[...] = (dot(hi_ref[...], back[...]) + dot(lo_ref[...], back[...])).astype(BF)
    for c in sent:
        c.wait_send()
    for d in range(1, n):
        @pl.when(i + d < n)
        def _():
            st_c[d].wait_send()
            tot_c[d].wait_send()


def store_kernel(mixer, blended, mixer_out, blended_out, sem):
    copies = [
        pltpu.make_async_copy(mixer, mixer_out, sem.at[0]),
        pltpu.make_async_copy(blended, blended_out, sem.at[1]),
    ]
    for c in copies:
        c.start()
    for c in copies:
        c.wait()


def per_device(
    queries, key_rows, value_rows, out_gate, log_decay, head_gain, out_weight,
    moe_input, moe_gain, expert_gate, expert_up, expert_down, route_ids, route_weights,
):
    n, shares = lax.axis_size("ep"), lax.axis_size("tp")
    tokens, top = route_ids.shape
    pairs = tokens * top
    cap = -(-2 * pairs // n // 16) * 16
    full = moe_input.shape[1]
    width = full // shares
    length, heads = log_decay.shape
    dim = head_gain.shape[1]
    hidden = expert_gate.shape[2]

    rows = n * cap
    quarter = length // shares
    vmem = pl.BlockSpec(memory_space=pltpu.VMEM)
    hbm = pl.BlockSpec(memory_space=pltpu.HBM)
    dma = pltpu.SemaphoreType.DMA
    mixer, blended = pl.pallas_call(
        functools.partial(layer_kernel, n, cap, heads),
        out_shape=(
            jax.ShapeDtypeStruct((quarter, full), BF),
            jax.ShapeDtypeStruct((tokens, width), BF),
        ),
        in_specs=[vmem] * 10 + [hbm] * 4,
        out_specs=(vmem, vmem),
        scratch_shapes=[
            pltpu.VMEM(out_weight.shape, BF),
            pltpu.VMEM((full, hidden), BF),
            pltpu.VMEM((full, hidden), BF),
            pltpu.VMEM((hidden, full), BF),
            pltpu.VMEM((4, rows, width), BF),
            pltpu.VMEM((4, rows, width), BF),
            pltpu.VMEM((2, rows, width), BF),
            pltpu.VMEM((rows, width), BF),
            pltpu.VMEM((rows, width), BF),
            pltpu.VMEM((rows, width), BF),
            pltpu.VMEM((rows, width), BF),
            pltpu.VMEM((heads * dim, dim), BF),
            pltpu.VMEM((n, heads * dim, dim), BF),
            pltpu.VMEM((8, dim), F32),
            pltpu.VMEM((n, 8, dim), F32),
            pltpu.VMEM((length, heads * dim), F32),
            pltpu.VMEM((length, heads * dim), BF),
            pltpu.VMEM((length, full), BF),
            pltpu.VMEM((2, quarter, full), BF),
            pltpu.VMEM((quarter, full), BF),
            pltpu.VMEM((quarter, full), BF),
            dma((4,)),
            dma((n,)), dma((n,)), dma((n,)), dma((n,)), dma((n,)), dma((n,)),
            dma((CHUNKS * PARTS, 3)), dma((CHUNKS * PARTS, 3)),
            dma((CHUNKS, 2)), dma((CHUNKS, 2)),
            dma((CHUNKS * PARTS,)), dma((CHUNKS * PARTS,)),
            dma((3,)), dma((3,)),
            dma((n,)), dma((n,)),
            pltpu.VMEM((rows, width), BF),
            pltpu.VMEM((tokens, rows), BF),
            pltpu.VMEM((tokens, rows), BF),
        ],
        compiler_params=pltpu.CompilerParams(
            collective_id=0, has_side_effects=True, vmem_limit_bytes=44 * 1024 * 1024
        ),
    )(
        queries, key_rows, value_rows, out_gate, log_decay, head_gain,
        moe_input, moe_gain.reshape(1, full), route_ids, route_weights,
        out_weight, expert_gate[0], expert_up[0], expert_down[0],
    )
    return pl.pallas_call(
        store_kernel,
        out_shape=(
            jax.ShapeDtypeStruct(mixer.shape, BF),
            jax.ShapeDtypeStruct(blended.shape, BF),
        ),
        in_specs=[vmem, vmem],
        out_specs=(hbm, hbm),
        scratch_shapes=[dma((2,))],
        compiler_params=pltpu.CompilerParams(vmem_limit_bytes=4 * 1024 * 1024),
    )(mixer, blended)


def solution(mesh):
    in_specs = (
        P("ep", "tp"),
        P("ep", "tp"),
        P("ep", "tp"),
        P("ep", "tp"),
        P("ep", "tp"),
        P("tp", None),
        P("tp", None),
        P("ep", None),
        P(),
        P("ep", None, "tp"),
        P("ep", None, "tp"),
        P("ep", "tp", None),
        P("ep", None),
        P("ep", None),
    )
    out_specs = (P(("ep", "tp"), None), P("ep", "tp"))
    return jax.shard_map(
        per_device, mesh=mesh, in_specs=in_specs, out_specs=out_specs, check_vma=False
    )
```

profile of v0, /device:TPU:0, one launch (start us, length us, event | category | flops | bytes accessed | tf_op | source)
XLA Modules:
  0.0 68.6 jit_solution(5299224652979638877)
XLA Ops:
  0.6 0.8 %copy.17.ids_ref = s32[128,2]{1,0:T(8,128)S(1)} copy(s32[128,2]{0,1:T(2,128)} %param.26) | data formatting | bytes 2048 | tf_op args[12]
  1.4 0.8 %copy.18.rw_ref = f32[128,2]{1,0:T(8,128)S(1)} copy(f32[128,2]{0,1:T(2,128)} %param.27) | data formatting | bytes 2048 | tf_op args[13]
  2.2 0.8 %copy.16.ld_ref = f32[256,2]{1,0:T(8,128)S(1)} copy(f32[256,2]{0,1:T(2,128)} %param.18) | data formatting | bytes 4096 | tf_op args[4]
  3.0 0.0 copy-start
  3.0 2.0 %copy-done = bf16[1,2048,896]{2,1,0:T(8,128)(2,1)S(1)} copy-done((bf16[1,2048,896]{2,1,0:T(8,128)(2,1)S(1)}, bf16[1,2048,896]{2,1,0:T(8,128)(2,1)}, u32[]{:S(2)}) %copy-start) | copy-done | bytes 3670040
  5.1 0.0 copy-start.1
  5.1 2.0 %copy-done.1 = bf16[1,2048,896]{2,1,0:T(8,128)(2,1)S(1)} copy-done((bf16[1,2048,896]{2,1,0:T(8,128)(2,1)S(1)}, bf16[1,2048,896]{2,1,0:T(8,128)(2,1)}, u32[]{:S(2)}) %copy-start.1) | copy-done | bytes 3670040
  7.1 0.0 copy-start.2
  7.1 1.2 %copy-done.2 = bf16[256,2048]{1,0:T(8,128)(2,1)S(1)} copy-done((bf16[256,2048]{1,0:T(8,128)(2,1)S(1)}, bf16[256,2048]{1,0:T(8,128)(2,1)}, u32[]{:S(2)}) %copy-start.2) | copy-done | bytes 1048600
  8.3 0.0 copy-start.3
  8.3 1.0 %copy-done.3 = bf16[128,2048]{1,0:T(8,128)(2,1)S(1)} copy-done((bf16[128,2048]{1,0:T(8,128)(2,1)S(1)}, bf16[128,2048]{1,0:T(8,128)(2,1)}, u32[]{:S(2)}) %copy-start.3) | copy-done | bytes 524312
  9.4 0.0 copy-start.4
  9.4 0.9 %copy-done.4 = bf16[256,256]{1,0:T(8,128)(2,1)S(1)} copy-done((bf16[256,256]{1,0:T(8,128)(2,1)S(1)}, bf16[256,256]{1,0:T(8,128)(2,1)}, u32[]{:S(2)}) %copy-start.4) | copy-done | bytes 131096
  10.3 0.0 copy-start.5
  10.3 0.9 %copy-done.5 = bf16[256,256]{1,0:T(8,128)(2,1)S(1)} copy-done((bf16[256,256]{1,0:T(8,128)(2,1)S(1)}, bf16[256,256]{1,0:T(8,128)(2,1)}, u32[]{:S(2)}) %copy-start.5) | copy-done | bytes 131096
  11.2 0.0 copy-start.6
  11.2 0.9 %copy-done.6 = bf16[256,256]{1,0:T(8,128)(2,1)S(1)} copy-done((bf16[256,256]{1,0:T(8,128)(2,1)S(1)}, bf16[256,256]{1,0:T(8,128)(2,1)}, u32[]{:S(2)}) %copy-start.6) | copy-done | bytes 131096
  12.1 0.0 copy-start.7
  12.1 0.9 %copy-done.7 = bf16[256,256]{1,0:T(8,128)(2,1)S(1)} copy-done((bf16[256,256]{1,0:T(8,128)(2,1)S(1)}, bf16[256,256]{1,0:T(8,128)(2,1)}, u32[]{:S(2)}) %copy-start.7) | copy-done | bytes 131096
  13.0 0.0 copy-start.8
  13.0 0.7 %copy-done.8 = f32[2048]{0:T(1024)S(1)} copy-done((f32[2048]{0:T(1024)S(1)}, f32[2048]{0:T(1024)}, u32[]{:S(2)}) %copy-start.8) | copy-done | bytes 8216
  13.7 0.0 copy-start.9
  13.7 0.7 copy-done.9
  14.4 53.4 %shard_map.149 = (bf16[64,2048]{1,0:T(8,128)(2,1)S(1)}, bf16[128,512]{1,0:T(8,128)(2,1)S(1)}) custom-call(bf16[256,256]{1,0:T(8,128)(2,1)S(1)} %copy-done.4, bf16[256,256]{1,0:T(8,128)(2,1)S(1)} %copy-done.5, bf16[256,256]{1,0:T(8,128)(2,1)S(1)} %copy-done.6, bf16[256,256]{1,0:T(8,128)(2,1)S(1)} %copy-done.7, f32[256,2]{1,0:T(8,128)S(1)} %copy.16.ld_ref, ...), custom_call_target="tpu_custom_call" | custom-call | tf_op jit(solution)/shard_map/pallas_call | solution.py:337
  67.8 0.8 %shard_map.150 = (bf16[64,2048]{1,0:T(8,128)(2,1)}, bf16[128,512]{1,0:T(8,128)(2,1)}) custom-call(bf16[64,2048]{1,0:T(8,128)(2,1)S(1)} %get-tuple-element.4.mixer, bf16[128,512]{1,0:T(8,128)(2,1)S(1)} %get-tuple-element.5.blended), custom_call_target="tpu_custom_call" | custom-call | tf_op jit(solution)/shard_map/pallas_call | solution.py:386
Async XLA Ops:
  3.0 2.0 %copy-start = (bf16[1,2048,896]{2,1,0:T(8,128)(2,1)S(1)}, bf16[1,2048,896]{2,1,0:T(8,128)(2,1)}, u32[]{:S(2)}) copy-start(bf16[1,2048,896]{2,1,0:T(8,128)(2,1)} %param.23) | copy-start | bytes 11010052
  5.1 2.0 %copy-start.1 = (bf16[1,2048,896]{2,1,0:T(8,128)(2,1)S(1)}, bf16[1,2048,896]{2,1,0:T(8,128)(2,1)}, u32[]{:S(2)}) copy-start(bf16[1,2048,896]{2,1,0:T(8,128)(2,1)} %param.24) | copy-start | bytes 11010052
  7.1 1.2 %copy-start.2 = (bf16[256,2048]{1,0:T(8,128)(2,1)S(1)}, bf16[256,2048]{1,0:T(8,128)(2,1)}, u32[]{:S(2)}) copy-start(bf16[256,2048]{1,0:T(8,128)(2,1)} %ow_hbm.1) | copy-start | bytes 3145732
  8.3 1.0 %copy-start.3 = (bf16[128,2048]{1,0:T(8,128)(2,1)S(1)}, bf16[128,2048]{1,0:T(8,128)(2,1)}, u32[]{:S(2)}) copy-start(bf16[128,2048]{1,0:T(8,128)(2,1)} %tok_ref.1) | copy-start | bytes 1572868
  9.4 0.9 %copy-start.4 = (bf16[256,256]{1,0:T(8,128)(2,1)S(1)}, bf16[256,256]{1,0:T(8,128)(2,1)}, u32[]{:S(2)}) copy-start(bf16[256,256]{1,0:T(8,128)(2,1)} %q_ref.1) | copy-start | bytes 393220
  10.3 0.9 %copy-start.5 = (bf16[256,256]{1,0:T(8,128)(2,1)S(1)}, bf16[256,256]{1,0:T(8,128)(2,1)}, u32[]{:S(2)}) copy-start(bf16[256,256]{1,0:T(8,128)(2,1)} %k_ref.1) | copy-start | bytes 393220
  11.2 0.9 %copy-start.6 = (bf16[256,256]{1,0:T(8,128)(2,1)S(1)}, bf16[256,256]{1,0:T(8,128)(2,1)}, u32[]{:S(2)}) copy-start(bf16[256,256]{1,0:T(8,128)(2,1)} %v_ref.1) | copy-start | bytes 393220
  12.1 0.9 %copy-start.7 = (bf16[256,256]{1,0:T(8,128)(2,1)S(1)}, bf16[256,256]{1,0:T(8,128)(2,1)}, u32[]{:S(2)}) copy-start(bf16[256,256]{1,0:T(8,128)(2,1)} %g_ref.1) | copy-start | bytes 393220
  13.0 0.7 %copy-start.8 = (f32[2048]{0:T(1024)S(1)}, f32[2048]{0:T(1024)}, u32[]{:S(2)}) copy-start(f32[2048]{0:T(1024)} %param.22) | copy-start | bytes 24580
  13.7 0.7 copy-start.9
where the time goes:
time: 69 us; the launch traced here: 68.6 us
  Pallas kernels  54.2 us (79%)
  local copies, waits for them, and re-layouts  13.7 us (20%)
    pallas_call x1, Pallas kernels, per_device(): pl.pallas_call(functools.partial(layer_kernel, n, cap, heads), out_shape=...  53.4 us
    unnamed x23, local copies, waits for them, and re-layouts  13.7 us

commit v1 on v0

--- a/solution.py
+++ b/solution.py
@@ -20,9 +20,10 @@
 
 def layer_kernel(
     n, cap, heads,
-    q_ref, k_ref, v_ref, g_ref, ld_ref, gain_ref, tok_ref, norm_ref, ids_ref, rw_ref,
+    tok_hbm, ids_hbm, norm_hbm, ld_hbm, k_hbm, v_hbm, q_hbm, rw_hbm, g_hbm, gain_hbm,
     ow_hbm, wg_hbm, wu_hbm, wd_hbm,
     mixer_ref, expert_ref,
+    tok_ref, ids_ref, norm_ref, ld_ref, k_ref, v_ref, q_ref, rw_ref, g_ref, gain_ref,
     ow, wg, wu, wd, x, part, near, half, far, done, back,
     st, st_in, tot, tot_in, inner, ho, mx, mr1, ms, mr2,
     w_sem, disp_s, disp_r, st_s, st_r, tot_s, tot_r, fwd_s, fwd_r,
@@ -58,7 +59,11 @@
 
     loads = [
         pltpu.make_async_copy(a, b, w_sem.at[m])
-        for m, (a, b) in enumerate(((ow_hbm, ow), (wg_hbm, wg), (wu_hbm, wu), (wd_hbm, wd)))
+        for m, (a, b) in enumerate((
+            (tok_hbm, tok_ref), (ids_hbm, ids_ref), (norm_hbm, norm_ref), (ld_hbm, ld_ref),
+            (k_hbm, k_ref), (v_hbm, v_ref), (q_hbm, q_ref), (rw_hbm, rw_ref), (g_hbm, g_ref),
+            (gain_hbm, gain_ref), (ow_hbm, ow), (wg_hbm, wg), (wu_hbm, wu), (wd_hbm, wd),
+        ))
     ]
     for c in loads:
         c.start()
@@ -68,30 +73,32 @@
     for peer in (j1, j2):
         pl.semaphore_signal(barrier, inc=1, device_id=(i, peer), device_id_type=pl.DeviceIdType.MESH)
 
-    tokens, top = ids_ref.shape
-    lanes = -(-n // 128) * 128
+    top, tokens = ids_ref.shape
+    lanes = -(-n // 16) * 16
+    loads[1].wait()
+    expert = lax.broadcasted_iota(jnp.int32, (lanes, tokens), 0)
+    named = [ids_ref[t : t + 1, :] == expert for t in range(top)]
+    strict = lax.broadcasted_iota(jnp.int32, (tokens, tokens), 0) < lax.broadcasted_iota(
+        jnp.int32, (tokens, tokens), 1
+    )
+    held = sum(jnp.where(m, 1.0, 0.0) for m in named)
+    before = dot(held.astype(BF), jnp.where(strict, 1.0, 0.0).astype(BF))
+    slot = lax.broadcasted_iota(jnp.int32, (rows, tokens), 0)
+    target = []
+    for t in range(top):
+        rank = jnp.sum(jnp.where(named[t], before, 0.0), axis=0, keepdims=True).astype(jnp.int32)
+        d = ids_ref[t : t + 1, :] - i
+        d = jnp.where(d < 0, d + n, d)
+        place = jnp.where(d == 0, 0, jnp.where(2 * d <= n, 2 * d - 1, 2 * (n - d)))
+        target.append(place * cap + rank)
+    pick = sum(jnp.where(slot == target[t], 1.0, 0.0) for t in range(top)).astype(BF)
+    loads[0].wait()
+    loads[2].wait()
     rows_f = tok_ref[...].astype(F32)
     scale = lax.rsqrt(jnp.mean(rows_f * rows_f, axis=-1, keepdims=True) + epsilon)
     mine = pl.ds(pl.multiple_of(j * width, width), width)
     normed = (tok_ref[:, mine].astype(F32) * scale * norm_ref[:, mine]).astype(BF)
-    expert = lax.broadcasted_iota(jnp.int32, (tokens, lanes), 1)
-    named = [ids_ref[:, t : t + 1] == expert for t in range(top)]
-    strict = lax.broadcasted_iota(jnp.int32, (tokens, tokens), 0) > lax.broadcasted_iota(
-        jnp.int32, (tokens, tokens), 1
-    )
-    held = sum(jnp.where(m, 1.0, 0.0) for m in named)
-    before = dot(jnp.where(strict, 1.0, 0.0).astype(BF), held.astype(BF))
-    slot = lax.broadcasted_iota(jnp.int32, (tokens, rows), 1)
-    pick, comb = 0.0, 0.0
-    for t in range(top):
-        rank = jnp.sum(jnp.where(named[t], before, 0.0), axis=1, keepdims=True).astype(jnp.int32)
-        d = ids_ref[:, t : t + 1] - i
-        d = jnp.where(d < 0, d + n, d)
-        place = jnp.where(d == 0, 0, jnp.where(2 * d <= n, 2 * d - 1, 2 * (n - d)))
-        hit = slot == place * cap + rank
-        pick = pick + jnp.where(hit, 1.0, 0.0)
-        comb = comb + jnp.where(hit, rw_ref[:, t : t + 1], 0.0)
-    piece = dot(pick.T.astype(BF), normed).astype(BF)
+    piece = dot(pick, normed).astype(BF)
     piece_ref[...] = piece
     x[0, 0:cap, :] = piece[0:cap]
     pl.semaphore_wait(barrier, n + 1)
@@ -105,20 +112,24 @@
         sent.append(disp[d])
 
     tot[...] = jnp.zeros_like(tot)
+    for c in loads[3:10]:
+        c.wait()
+    comb = sum(jnp.where(slot == target[t], rw_ref[t : t + 1, :], 0.0) for t in range(top)).T
     hi = comb.astype(BF)
     hi_ref[...] = hi
     lo_ref[...] = (comb - hi.astype(F32)).astype(BF)
     causal = lax.broadcasted_iota(jnp.int32, (length, length), 0) >= lax.broadcasted_iota(
         jnp.int32, (length, length), 1
     )
-    lower = jnp.where(causal, 1.0, 0.0)
-    cum = [
-        lax.dot_general(
-            lower, jnp.broadcast_to(ld_ref[:, h : h + 1], (length, dim)), (((1,), (0,)), ((), ())),
-            precision=lax.Precision.HIGHEST, preferred_element_type=F32,
-        )
-        for h in range(heads)
-    ]
+    upper = jnp.where(
+        lax.broadcasted_iota(jnp.int32, (length, length), 0)
+        <= lax.broadcasted_iota(jnp.int32, (length, length), 1), 1.0, 0.0
+    )
+    level = lax.dot_general(
+        ld_ref[...], upper, (((1,), (0,)), ((), ())),
+        precision=lax.Precision.HIGHEST, preferred_element_type=F32,
+    )
+    cum = [jnp.broadcast_to(level[h : h + 1, :], (dim, length)).T for h in range(heads)]
 
     for h in range(heads):
         c = slice(h * dim, (h + 1) * dim)
@@ -163,14 +174,13 @@
     for h in range(heads):
         c = slice(h * dim, (h + 1) * dim)
         scores = dot(q_ref[:, c], k_ref[:, c], (((1,), (1,)), ((), ()))) * dim ** (-0.5)
-        spread = jnp.where(causal, cum[h][:, 0:1] - cum[h].T[0:1, :], -jnp.inf)
+        spread = jnp.where(causal, cum[h][:, 0:1] - level[h : h + 1, :], -jnp.inf)
         inner[:, c] = dot((scores * jnp.exp(spread)).astype(BF), v_ref[:, c])
 
     for u in range(PARTS):
         forward(PARTS + u)
         relay(u)
-    loads[0].wait()
-    for c in loads[1:]:
+    for c in loads[10:]:
         c.wait()
 
     def stripe(m):
@@ -334,15 +344,20 @@
     vmem = pl.BlockSpec(memory_space=pltpu.VMEM)
     hbm = pl.BlockSpec(memory_space=pltpu.HBM)
     dma = pltpu.SemaphoreType.DMA
+    args = (
+        moe_input, route_ids.T, moe_gain.reshape(1, full), log_decay.T, key_rows, value_rows, queries,
+        route_weights.T, out_gate, head_gain, out_weight, expert_gate[0], expert_up[0], expert_down[0],
+    )
+    args = [pltpu.with_memory_space_constraint(a, pltpu.HBM) for a in args]
     mixer, blended = pl.pallas_call(
         functools.partial(layer_kernel, n, cap, heads),
         out_shape=(
-            jax.ShapeDtypeStruct((quarter, full), BF),
-            jax.ShapeDtypeStruct((tokens, width), BF),
+            pltpu.VMEM((quarter, full), BF),
+            pltpu.VMEM((tokens, width), BF),
         ),
-        in_specs=[vmem] * 10 + [hbm] * 4,
+        in_specs=[hbm] * len(args),
         out_specs=(vmem, vmem),
-        scratch_shapes=[
+        scratch_shapes=[pltpu.VMEM(a.shape, a.dtype) for a in args[:10]] + [
             pltpu.VMEM(out_weight.shape, BF),
             pltpu.VMEM((full, hidden), BF),
             pltpu.VMEM((full, hidden), BF),
@@ -364,7 +379,7 @@
             pltpu.VMEM((2, quarter, full), BF),
             pltpu.VMEM((quarter, full), BF),
             pltpu.VMEM((quarter, full), BF),
-            dma((4,)),
+            dma((len(args),)),
             dma((n,)), dma((n,)), dma((n,)), dma((n,)), dma((n,)), dma((n,)),
             dma((CHUNKS * PARTS, 3)), dma((CHUNKS * PARTS, 3)),
             dma((CHUNKS, 2)), dma((CHUNKS, 2)),
@@ -376,13 +391,9 @@
             pltpu.VMEM((tokens, rows), BF),
         ],
         compiler_params=pltpu.CompilerParams(
-            collective_id=0, has_side_effects=True, vmem_limit_bytes=44 * 1024 * 1024
+            collective_id=0, has_side_effects=True, vmem_limit_bytes=56 * 1024 * 1024
         ),
-    )(
-        queries, key_rows, value_rows, out_gate, log_decay, head_gain,
-        moe_input, moe_gain.reshape(1, full), route_ids, route_weights,
-        out_weight, expert_gate[0], expert_up[0], expert_down[0],
-    )
+    )(*args)
     return pl.pallas_call(
         store_kernel,
         out_shape=(

time: 69 us -> 54.5 us (0.79)
  local copies, waits for them, and re-layouts: 13.7 us -> 0 us
    unnamed x23 -> x0, local copies, waits for them, and re-layouts: 13.7 us -> none
where the time goes in v1:
time: 54.5 us; the launch traced here: 54.4 us
  Pallas kernels  53.7 us (99%)
  between operations  0.64 us (1%)
    pallas_call x1, Pallas kernels, per_device(): pl.pallas_call(functools.partial(layer_kernel, n, cap, heads), out_shape=...  53 us

profile of v1, /device:TPU:0, one launch (start us, length us, event | category | flops | bytes accessed | tf_op | source)
XLA Modules:
  0.0 54.4 jit_solution(5600229824351648493)
XLA Ops:
  0.6 53.0 %shard_map.149 = (bf16[64,2048]{1,0:T(8,128)(2,1)S(1)}, bf16[128,512]{1,0:T(8,128)(2,1)S(1)}) custom-call(bf16[128,2048]{1,0:T(8,128)(2,1)} %tok_hbm.1, s32[2,128]{1,0:T(2,128)} %bitcast.12, f32[1,2048]{1,0:T(1,128)} %bitcast.10, f32[2,256]{1,0:T(2,128)} %bitcast.11, bf16[256,256]{1,0:T(8,128)(2,1)} %k_hbm.1, bf16[256,256]{1,0:T(8,128)(2,1)} %v_hbm.1, ...), custom_call_target="tpu_custom_call" | custom-call | tf_op jit(solution)/shard_map/pallas_call | solution.py:352
  53.6 0.8 %shard_map.150 = (bf16[64,2048]{1,0:T(8,128)(2,1)}, bf16[128,512]{1,0:T(8,128)(2,1)}) custom-call(bf16[64,2048]{1,0:T(8,128)(2,1)S(1)} %get-tuple-element.4.mixer, bf16[128,512]{1,0:T(8,128)(2,1)S(1)} %get-tuple-element.5.blended), custom_call_target="tpu_custom_call" | custom-call | tf_op jit(solution)/shard_map/pallas_call | solution.py:397

commit v2 on v1

v2 whole, which is shorter than its diff:
```python
import functools

import jax
import jax.numpy as jnp
from jax import lax
from jax.experimental import pallas as pl
from jax.experimental.pallas import tpu as pltpu
from jax.sharding import PartitionSpec as P

epsilon = 1e-06
CHUNKS = 4
PIECES = 8
BF = jnp.bfloat16
F32 = jnp.float32


def dot(a, b, dims=(((1,), (0,)), ((), ()))):
    return lax.dot_general(a, b, dims, preferred_element_type=F32)


def layer_kernel(
    n, cap, heads,
    tok_hbm, ids_hbm, norm_hbm, ld_hbm, k_hbm, v_hbm, q_hbm, rw_hbm, g_hbm, gain_hbm,
    ow_hbm, wg_hbm, wu_hbm, wd_hbm,
    mixer_ref, expert_ref,
    tok_ref, ids_ref, norm_ref, ld_ref, k_ref, v_ref, q_ref, rw_ref, g_ref, gain_ref,
    ow, wg, wu, wd, x, part, near, half, far, done, back,
    st, st_in, tot, tot_in, window, enter, inner, ho, mx, mr1, ms, mr2,
    w_sem, disp_s, disp_r, both_s, both_r, st_s, st_r, tot_s, tot_r, y_s, y_r, c_s, c_r,
    red_s, red_r, redy_s, redy_r, mix_s, mix_r, ret_s, ret_r,
    piece_ref, both_ref, hi_ref, lo_ref,
):
    i, j = lax.axis_index("ep"), lax.axis_index("tp")
    j1 = j + 1 - 2 * lax.rem(j, 2)
    j2 = lax.rem(j + 2, 4)
    j3 = lax.rem(j1 + 2, 4)
    places = (j, j1, j2, j3)
    rows = n * cap
    step = rows // CHUNKS
    small = rows // PIECES
    width = x.shape[2]
    dim = gain_ref.shape[1]
    length = q_ref.shape[0]
    quarter = length // 4
    rounds = n.bit_length() - 1

    def partner(d):
        r = i
        for b in range(rounds):
            if (d >> b) & 1:
                r = r + (1 << b) * (1 - 2 * lax.rem(lax.div(i, 1 << b), 2))
        return r

    def position(d):
        return (((d >> 1) & 1) * 2 + d // (n // 2)) * (n // 4) + ((d % (n // 2)) >> 2) * 2 + (d & 1)

    offsets = sorted(range(n), key=position)

    def members(p):
        return [d for d in offsets[p * n // PIECES : (p + 1) * n // PIECES]]

    def slots(d):
        return pl.ds(position(d) * cap, cap)

    def chunk(g):
        return pl.ds(g * step, step)

    def bit(p):
        return pl.ds(p * small, small)

    def of(g):
        return range(g * PIECES // CHUNKS, (g + 1) * PIECES // CHUNKS)

    def across(g):
        return g % 2 == 1

    def send(src, dst, ss, rs, dev):
        return pltpu.make_async_remote_copy(
            src_ref=src, dst_ref=dst, send_sem=ss, recv_sem=rs, device_id=dev,
            device_id_type=pl.DeviceIdType.MESH,
        )

    loads = [
        pltpu.make_async_copy(a, b, w_sem.at[m])
        for m, (a, b) in enumerate((
            (tok_hbm, tok_ref), (ids_hbm, ids_ref), (norm_hbm, norm_ref), (ld_hbm, ld_ref),
            (k_hbm, k_ref), (v_hbm, v_ref), (q_hbm, q_ref), (rw_hbm, rw_ref), (g_hbm, g_ref),
            (gain_hbm, gain_ref), (ow_hbm, ow), (wg_hbm, wg), (wu_hbm, wu), (wd_hbm, wd),
        ))
    ]
    for c in loads:
        c.start()
    barrier = pltpu.get_barrier_semaphore()
    for d in range(1, n):
        pl.semaphore_signal(barrier, inc=1, device_id=(partner(d), j), device_id_type=pl.DeviceIdType.MESH)
    for peer in (j1, j2):
        pl.semaphore_signal(barrier, inc=1, device_id=(i, peer), device_id_type=pl.DeviceIdType.MESH)

    def block(m):
        return pl.ds(pl.multiple_of(places[m] * width, width), width)

    top, tokens = ids_ref.shape
    lanes = -(-n // 16) * 16
    loads[1].wait()
    expert = lax.broadcasted_iota(jnp.int32, (lanes, tokens), 0)
    named = [ids_ref[t : t + 1, :] == expert for t in range(top)]
    strict = lax.broadcasted_iota(jnp.int32, (tokens, tokens), 0) < lax.broadcasted_iota(
        jnp.int32, (tokens, tokens), 1
    )
    held = sum(jnp.where(m, 1.0, 0.0) for m in named)
    before = dot(held.astype(BF), jnp.where(strict, 1.0, 0.0).astype(BF))
    slot = lax.broadcasted_iota(jnp.int32, (rows, tokens), 0)
    target = []
    for t in range(top):
        rank = jnp.sum(jnp.where(named[t], before, 0.0), axis=0, keepdims=True).astype(jnp.int32)
        d = jnp.bitwise_xor(ids_ref[t : t + 1, :], i)
        over = jnp.where(d >= n // 2, 1, 0)
        kept = d - over * (n // 2)
        place = ((d >> 1) & 1) * 2 + over
        place = place * (n // 4) + (kept >> 2) * 2 + (d & 1)
        target.append(place * cap + rank)
    pick = sum(jnp.where(slot == target[t], 1.0, 0.0) for t in range(top)).astype(BF)
    loads[0].wait()
    loads[2].wait()
    rows_f = tok_ref[...].astype(F32)
    scale = lax.rsqrt(jnp.mean(rows_f * rows_f, axis=-1, keepdims=True) + epsilon)

    def normed(m):
        return (tok_ref[:, block(m)].astype(F32) * scale * norm_ref[:, block(m)]).astype(BF)

    piece = dot(pick, normed(0)).astype(BF)
    piece_ref[...] = piece
    x[0, 0:cap, :] = piece[0:cap]
    both = normed(2)
    for g in range(0, CHUNKS, 2):
        both_ref[chunk(g), :] = dot(pick[g * step : (g + 1) * step], both).astype(BF)
    x[2, 0:cap, :] = both_ref[0:cap, :]
    pl.semaphore_wait(barrier, n + 1)

    sent = []
    disp, disp2 = [None] * n, [None] * n
    for d in range(1, n):
        disp[d] = send(piece_ref.at[slots(d)], x.at[0, slots(d)], disp_s.at[d], disp_r.at[d], (partner(d), j))
        sent.append(disp[d])
        if d < n // 2:
            disp2[d] = send(both_ref.at[slots(d)], x.at[2, slots(d)], both_s.at[d], both_r.at[d], (partner(d), j))
            sent.append(disp2[d])

    def dispatch(g):
        for p in of(g):
            for d in members(p):
                if d:
                    disp[d].start()
                    if not across(g):
                        disp2[d].start()

    dispatch(1)
    dispatch(0)

    y_c, c0_c, c2_c = [], [], []
    for p in range(PIECES):
        r = bit(p)
        y_c.append(send(x.at[0, r], x.at[2, r], y_s.at[p], y_r.at[p], (i, j2)))
        c0_c.append(send(x.at[0, r], x.at[1, r], c_s.at[p, 0], c_r.at[p, 0], (i, j1)))
        c2_c.append(send(x.at[2, r], x.at[3, r], c_s.at[p, 1], c_r.at[p, 1], (i, j1)))
        sent += [c0_c[p], c2_c[p]]
        if across(p * CHUNKS // PIECES):
            sent.append(y_c[p])

    def forward(g, which=None):
        for p in of(g) if which is None else [of(g)[which]]:
            for d in members(p):
                if d:
                    disp[d].wait_recv()
                    if not across(g):
                        disp2[d].wait_recv()
            if across(g):
                y_c[p].start()
            else:
                c2_c[p].start()
            c0_c[p].start()

    def relay(g):
        for p in of(g):
            y_c[p].wait_recv()
            c2_c[p].start()

    causal = lax.broadcasted_iota(jnp.int32, (length, length), 0) >= lax.broadcasted_iota(
        jnp.int32, (length, length), 1
    )
    upper = jnp.where(
        lax.broadcasted_iota(jnp.int32, (length, length), 0)
        <= lax.broadcasted_iota(jnp.int32, (length, length), 1), 1.0, 0.0
    )
    for c in loads[3:10]:
        c.wait()
    level = lax.dot_general(
        ld_ref[...], upper, (((1,), (0,)), ((), ())),
        precision=lax.Precision.HIGHEST, preferred_element_type=F32,
    )
    cum = [jnp.broadcast_to(level[h : h + 1, :], (dim, length)).T for h in range(heads)]
    tot[0] = jnp.zeros(tot.shape[1:], F32)
    for h in range(heads):
        c = slice(h * dim, (h + 1) * dim)
        total = cum[h][length - 1 : length, :]
        keys = k_ref[:, c].astype(F32) * jnp.exp(total - cum[h])
        window[c, :] = dot(keys.T.astype(BF), v_ref[:, c])
        tot[0, h : h + 1, :] = total
    st[0] = window[...].astype(BF)
    enter[...] = jnp.zeros_like(enter)
    st_c, tot_c = [], []
    for r in range(rounds):
        later = (lax.rem(i + (1 << r), n), j)
        st_c.append(send(st.at[r], st_in.at[r], st_s.at[r], st_r.at[r], later))
        tot_c.append(send(tot.at[r], tot_in.at[r], tot_s.at[r], tot_r.at[r], later))

    def pass_on(r):
        @pl.when(i + (1 << r) < n)
        def _():
            st_c[r].start()
            tot_c[r].start()

    span = [jnp.zeros(tot.shape[1:], F32)]

    def spread_rows(totals):
        return jnp.concatenate(
            [jnp.broadcast_to(jnp.exp(totals[h : h + 1, :]), (dim, dim)) for h in range(heads)], axis=0
        )

    def absorb(r):
        @pl.when(i >= 1 << r)
        def _():
            st_c[r].wait_recv()
            tot_c[r].wait_recv()

        @pl.when(i < 1 << r)
        def _():
            st_in[r] = jnp.zeros(st_in.shape[1:], BF)
            tot_in[r] = jnp.zeros(tot_in.shape[1:], F32)

        arrived = st_in[r].astype(F32)
        enter[...] = spread_rows(span[0]) * arrived + enter[...]
        span[0] = span[0] + tot_in[r]
        if r + 1 < rounds:
            window[...] = spread_rows(tot[r]) * arrived + window[...]
            st[r + 1] = window[...].astype(BF)
            tot[r + 1] = tot[r] + tot_in[r]
            pass_on(r + 1)

    pass_on(0)
    dispatch(2)
    dispatch(3)

    for h in range(heads):
        c = slice(h * dim, (h + 1) * dim)
        scores = dot(q_ref[:, c], k_ref[:, c], (((1,), (1,)), ((), ()))) * dim ** (-0.5)
        spread = jnp.where(causal, cum[h][:, 0:1] - level[h : h + 1, :], -jnp.inf)
        inner[:, c] = dot((scores * jnp.exp(spread)).astype(BF), v_ref[:, c])

    def stripe(m):
        return pl.ds(pl.multiple_of(places[m] * quarter, quarter), quarter)

    mix_a = send(mx.at[stripe(1)], mr1.at[0], mix_s.at[0], mix_r.at[0], (i, j1))
    mix_b = send(mx.at[stripe(3)], mr1.at[1], mix_s.at[1], mix_r.at[1], (i, j1))
    mix_c = send(ms, mr2, mix_s.at[2], mix_r.at[2], (i, j2))
    sent += [mix_a, mix_b, mix_c]

    def retention():
        entering = enter[...].astype(BF)
        for h in range(heads):
            c = slice(h * dim, (h + 1) * dim)
            queries = (q_ref[:, c].astype(F32) * jnp.exp(cum[h])).astype(BF)
            kept = inner[:, c] + dot(queries, entering[h * dim : (h + 1) * dim, :])
            unit = kept * lax.rsqrt(jnp.mean(kept * kept, axis=-1, keepdims=True) + epsilon)
            ho[:, c] = (unit * gain_ref[h : h + 1, :] * jax.nn.silu(g_ref[:, c].astype(F32))).astype(BF)
        mx[...] = dot(ho[...], ow[...]).astype(BF)
        mix_b.start()
        mix_a.start()

    def mix_cross():
        mix_b.wait_recv()
        ms[...] = (mx[stripe(2), :].astype(F32) + mr1[1].astype(F32)).astype(BF)

    red, red_y = [], []
    for g in range(CHUNKS):
        r = chunk(g)
        red.append((
            send(part.at[1, r], near.at[0, r], red_s.at[g, 0], red_r.at[g, 0], (i, j1)),
            send(part.at[3, r], near.at[1, r], red_s.at[g, 1], red_r.at[g, 1], (i, j1)),
        ))
        sent += list(red[-1])
    for p in range(PIECES):
        r = bit(p)
        red_y.append(send(half.at[r], far.at[r], redy_s.at[p], redy_r.at[p], (i, j2)))
    sent += red_y

    def experts(g, between=None, after=None):
        r = chunk(g)
        gate, up = 0.0, 0.0
        for m in (0, 2, 1, 3):
            if m == 1:
                if between is not None:
                    between()
                for p in of(g):
                    c0_c[p].wait_recv()
                    c2_c[p].wait_recv()
            gate = gate + dot(x[m, r, :], wg[block(m), :])
            up = up + dot(x[m, r, :], wu[block(m), :])
        hidden = (jax.nn.silu(gate) * up).astype(BF)
        if after is not None:
            after()
        for m in (3, 1, 2, 0):
            part[m, r, :] = dot(hidden, wd[:, block(m)]).astype(BF)
            if m == 3:
                red[g][1].start()
            if m == 1:
                red[g][0].start()
        cross(g)

    def cross(g):
        red[g][1].wait_recv()
        for p in of(g):
            r = bit(p)
            half[r, :] = (part[2, r, :].astype(F32) + near[1, r, :].astype(F32)).astype(BF)
            red_y[p].start()

    ret = [None] * n
    for d in range(1, n):
        ret[d] = send(done.at[slots(d)], back.at[slots(d)], ret_s.at[d], ret_r.at[d], (partner(d), j))
        sent.append(ret[d])

    def home(g, which=None):
        if not which:
            red[g][0].wait_recv()
        for p in of(g) if which is None else [of(g)[which]]:
            r = bit(p)
            red_y[p].wait_recv()
            done[r, :] = (
                part[0, r, :].astype(F32) + near[0, r, :].astype(F32) + far[r, :].astype(F32)
            ).astype(BF)
            for d in members(p):
                if d:
                    ret[d].start()
                else:
                    back[0:cap, :] = done[0:cap, :]

    forward(0)
    for c in loads[10:]:
        c.wait()
    experts(0, after=lambda: forward(1))
    absorb(0)
    comb = sum(jnp.where(slot == target[t], rw_ref[t : t + 1, :], 0.0) for t in range(top)).T
    hi = comb.astype(BF)
    hi_ref[...] = hi
    lo_ref[...] = (comb - hi.astype(F32)).astype(BF)
    forward(2)
    relay(1)
    forward(3, 0)
    experts(1, after=lambda: forward(3, 1))
    for r in range(1, rounds - 1):
        absorb(r)
    experts(2)
    home(0)
    relay(3)
    experts(3, after=lambda: home(1, 0))
    home(1, 1)
    absorb(rounds - 1)
    retention()
    home(2)
    home(3, 0)
    mix_cross()
    mix_c.start()
    home(3, 1)

    def gather(g):
        for p in of(g):
            for d in members(p):
                if d:
                    ret[d].wait_recv()
        c = slice(g * step, (g + 1) * step)
        return dot(hi_ref[:, c], back[c, :]) + dot(lo_ref[:, c], back[c, :])

    blend = gather(0) + gather(2) + gather(1)
    mix_a.wait_recv()
    mix_c.wait_recv()
    mixer_ref[...] = (
        mx[stripe(0), :].astype(F32) + mr1[0].astype(F32) + mr2[...].astype(F32)
    ).astype(BF)
    expert_ref[...] = (blend + gather(3)).astype(BF)
    for c in sent:
        c.wait_send()
    for r in range(rounds):
        @pl.when(i + (1 << r) < n)
        def _():
            st_c[r].wait_send()
            tot_c[r].wait_send()


def store_kernel(mixer, blended, mixer_out, blended_out, sem):
    copies = [
        pltpu.make_async_copy(mixer, mixer_out, sem.at[0]),
        pltpu.make_async_copy(blended, blended_out, sem.at[1]),
    ]
    for c in copies:
        c.start()
    for c in copies:
        c.wait()


def per_device(
    queries, key_rows, value_rows, out_gate, log_decay, head_gain, out_weight,
    moe_input, moe_gain, expert_gate, expert_up, expert_down, route_ids, route_weights,
):
    n, shares = lax.axis_size("ep"), lax.axis_size("tp")
    tokens, top = route_ids.shape
    pairs = tokens * top
    cap = -(-2 * pairs // n // 16) * 16
    full = moe_input.shape[1]
    width = full // shares
    length, heads = log_decay.shape
    dim = head_gain.shape[1]
    hidden = expert_gate.shape[2]

    rows = n * cap
    rounds = n.bit_length() - 1
    quarter = length // shares
    vmem = pl.BlockSpec(memory_space=pltpu.VMEM)
    hbm = pl.BlockSpec(memory_space=pltpu.HBM)
    dma = pltpu.SemaphoreType.DMA
    args = (
        moe_input, route_ids.T, moe_gain.reshape(1, full), log_decay.T, key_rows, value_rows, queries,
        route_weights.T, out_gate, head_gain, out_weight, expert_gate[0], expert_up[0], expert_down[0],
    )
    args = [pltpu.with_memory_space_constraint(a, pltpu.HBM) for a in args]
    mixer, blended = pl.pallas_call(
        functools.partial(layer_kernel, n, cap, heads),
        out_shape=(
            pltpu.VMEM((quarter, full), BF),
            pltpu.VMEM((tokens, width), BF),
        ),
        in_specs=[hbm] * len(args),
        out_specs=(vmem, vmem),
        scratch_shapes=[pltpu.VMEM(a.shape, a.dtype) for a in args[:10]] + [
            pltpu.VMEM(out_weight.shape, BF),
            pltpu.VMEM((full, hidden), BF),
            pltpu.VMEM((full, hidden), BF),
            pltpu.VMEM((hidden, full), BF),
            pltpu.VMEM((4, rows, width), BF),
            pltpu.VMEM((4, rows, width), BF),
            pltpu.VMEM((2, rows, width), BF),
            pltpu.VMEM((rows, width), BF),
            pltpu.VMEM((rows, width), BF),
            pltpu.VMEM((rows, width), BF),
            pltpu.VMEM((rows, width), BF),
            pltpu.VMEM((rounds, heads * dim, dim), BF),
            pltpu.VMEM((rounds, heads * dim, dim), BF),
            pltpu.VMEM((rounds, 8, dim), F32),
            pltpu.VMEM((rounds, 8, dim), F32),
            pltpu.VMEM((heads * dim, dim), F32),
            pltpu.VMEM((heads * dim, dim), F32),
            pltpu.VMEM((length, heads * dim), F32),
            pltpu.VMEM((length, heads * dim), BF),
            pltpu.VMEM((length, full), BF),
            pltpu.VMEM((2, quarter, full), BF),
            pltpu.VMEM((quarter, full), BF),
            pltpu.VMEM((quarter, full), BF),
            dma((len(args),)),
            dma((n,)), dma((n,)), dma((n,)), dma((n,)),
            dma((rounds,)), dma((rounds,)), dma((rounds,)), dma((rounds,)),
            dma((PIECES,)), dma((PIECES,)), dma((PIECES, 2)), dma((PIECES, 2)),
            dma((CHUNKS, 2)), dma((CHUNKS, 2)),
            dma((PIECES,)), dma((PIECES,)),
            dma((3,)), dma((3,)),
            dma((n,)), dma((n,)),
            pltpu.VMEM((rows, width), BF),
            pltpu.VMEM((rows, width), BF),
            pltpu.VMEM((tokens, rows), BF),
            pltpu.VMEM((tokens, rows), BF),
        ],
        compiler_params=pltpu.CompilerParams(
            collective_id=0, has_side_effects=True, vmem_limit_bytes=56 * 1024 * 1024
        ),
    )(*args)
    return pl.pallas_call(
        store_kernel,
        out_shape=(
            jax.ShapeDtypeStruct(mixer.shape, BF),
            jax.ShapeDtypeStruct(blended.shape, BF),
        ),
        in_specs=[vmem, vmem],
        out_specs=(hbm, hbm),
        scratch_shapes=[dma((2,))],
        compiler_params=pltpu.CompilerParams(vmem_limit_bytes=4 * 1024 * 1024),
    )(mixer, blended)


def solution(mesh):
    in_specs = (
        P("ep", "tp"),
        P("ep", "tp"),
        P("ep", "tp"),
        P("ep", "tp"),
        P("ep", "tp"),
        P("tp", None),
        P("tp", None),
        P("ep", None),
        P(),
        P("ep", None, "tp"),
        P("ep", None, "tp"),
        P("ep", "tp", None),
        P("ep", None),
        P("ep", None),
    )
    out_specs = (P(("ep", "tp"), None), P("ep", "tp"))
    return jax.shard_map(
        per_device, mesh=mesh, in_specs=in_specs, out_specs=out_specs, check_vma=False
    )
```

time: 54.5 us -> 43.5 us (0.80)
  Pallas kernels: 53.7 us -> 42.7 us
    pallas_call x1, Pallas kernels: 53 us -> 41.9 us  [per_device(): pl.pallas_call(functools.partial(layer_kernel, n, cap, heads), out_shape=...]
where the time goes in v2:
time: 43.5 us; the launch traced here: 43.3 us
  Pallas kernels  42.7 us (98%)
  between operations  0.64 us (1%)
    pallas_call x1, Pallas kernels, per_device(): pl.pallas_call(functools.partial(layer_kernel, n, cap, heads), out_shape=...  41.9 us

profile of v2, /device:TPU:0, one launch (start us, length us, event | category | flops | bytes accessed | tf_op | source)
XLA Modules:
  0.0 43.3 jit_solution(4225718283028239969)
XLA Ops:
  0.6 41.9 %shard_map.149 = (bf16[64,2048]{1,0:T(8,128)(2,1)S(1)}, bf16[128,512]{1,0:T(8,128)(2,1)S(1)}) custom-call(bf16[128,2048]{1,0:T(8,128)(2,1)} %tok_hbm.1, s32[2,128]{1,0:T(2,128)} %bitcast.12, f32[1,2048]{1,0:T(1,128)} %bitcast.10, f32[2,256]{1,0:T(2,128)} %bitcast.11, bf16[256,256]{1,0:T(8,128)(2,1)} %k_hbm.1, bf16[256,256]{1,0:T(8,128)(2,1)} %v_hbm.1, ...), custom_call_target="tpu_custom_call" | custom-call | tf_op jit(solution)/shard_map/pallas_call | solution.py:435
  42.6 0.8 %shard_map.150 = (bf16[64,2048]{1,0:T(8,128)(2,1)}, bf16[128,512]{1,0:T(8,128)(2,1)}) custom-call(bf16[64,2048]{1,0:T(8,128)(2,1)S(1)} %get-tuple-element.4.mixer, bf16[128,512]{1,0:T(8,128)(2,1)S(1)} %get-tuple-element.5.blended), custom_call_target="tpu_custom_call" | custom-call | tf_op jit(solution)/shard_map/pallas_call | solution.py:484

commit v3 on v2

--- a/solution.py
+++ b/solution.py
@@ -20,14 +20,13 @@
 
 def layer_kernel(
     n, cap, heads,
-    tok_hbm, ids_hbm, norm_hbm, ld_hbm, k_hbm, v_hbm, q_hbm, rw_hbm, g_hbm, gain_hbm,
+    tok_hbm, ids_hbm, norm_hbm, ld_hbm, rw_hbm, gain_hbm, k_hbm, v_hbm, q_hbm, g_hbm,
     ow_hbm, wg_hbm, wu_hbm, wd_hbm,
     mixer_ref, expert_ref,
-    tok_ref, ids_ref, norm_ref, ld_ref, k_ref, v_ref, q_ref, rw_ref, g_ref, gain_ref,
+    tok_ref, ids_ref, norm_ref, ld_ref, rw_ref, gain_ref, kvqg,
     ow, wg, wu, wd, x, part, near, half, far, done, back,
     st, st_in, tot, tot_in, window, enter, inner, ho, mx, mr1, ms, mr2,
-    w_sem, disp_s, disp_r, both_s, both_r, st_s, st_r, tot_s, tot_r, y_s, y_r, c_s, c_r,
-    red_s, red_r, redy_s, redy_r, mix_s, mix_r, ret_s, ret_r,
+    w_sem, sent_s, disp_r, st_s, st_r, tot_s, tot_r, y_r, c_r, red_r, redy_r, mix_r, ret_r,
     piece_ref, both_ref, hi_ref, lo_ref,
 ):
     i, j = lax.axis_index("ep"), lax.axis_index("tp")
@@ -40,7 +39,8 @@
     small = rows // PIECES
     width = x.shape[2]
     dim = gain_ref.shape[1]
-    length = q_ref.shape[0]
+    k_ref, v_ref, q_ref, g_ref = [kvqg.at[m] for m in range(4)]
+    length = kvqg.shape[1]
     quarter = length // 4
     rounds = n.bit_length() - 1
 
@@ -80,15 +80,22 @@
             device_id_type=pl.DeviceIdType.MESH,
         )
 
-    loads = [
+    DISPATCH, BOTH, ACROSS, CORE, HALVES, SUMS, MIX, HOME = range(8)
+    small_loads = [
         pltpu.make_async_copy(a, b, w_sem.at[m])
         for m, (a, b) in enumerate((
             (tok_hbm, tok_ref), (ids_hbm, ids_ref), (norm_hbm, norm_ref), (ld_hbm, ld_ref),
-            (k_hbm, k_ref), (v_hbm, v_ref), (q_hbm, q_ref), (rw_hbm, rw_ref), (g_hbm, g_ref),
-            (gain_hbm, gain_ref), (ow_hbm, ow), (wg_hbm, wg), (wu_hbm, wu), (wd_hbm, wd),
+            (rw_hbm, rw_ref), (gain_hbm, gain_ref),
         ))
     ]
-    for c in loads:
+    head_loads = [
+        pltpu.make_async_copy(a, kvqg.at[m], w_sem.at[6]) for m, a in enumerate((k_hbm, v_hbm, q_hbm, g_hbm))
+    ]
+    weight_loads = [
+        pltpu.make_async_copy(a, b, w_sem.at[7 + m])
+        for m, (a, b) in enumerate(((ow_hbm, ow), (wg_hbm, wg), (wu_hbm, wu), (wd_hbm, wd)))
+    ]
+    for c in small_loads + head_loads + weight_loads:
         c.start()
     barrier = pltpu.get_barrier_semaphore()
     for d in range(1, n):
@@ -101,7 +108,7 @@
 
     top, tokens = ids_ref.shape
     lanes = -(-n // 16) * 16
-    loads[1].wait()
+    small_loads[1].wait()
     expert = lax.broadcasted_iota(jnp.int32, (lanes, tokens), 0)
     named = [ids_ref[t : t + 1, :] == expert for t in range(top)]
     strict = lax.broadcasted_iota(jnp.int32, (tokens, tokens), 0) < lax.broadcasted_iota(
@@ -120,8 +127,8 @@
         place = place * (n // 4) + (kept >> 2) * 2 + (d & 1)
         target.append(place * cap + rank)
     pick = sum(jnp.where(slot == target[t], 1.0, 0.0) for t in range(top)).astype(BF)
-    loads[0].wait()
-    loads[2].wait()
+    small_loads[0].wait()
+    small_loads[2].wait()
     rows_f = tok_ref[...].astype(F32)
     scale = lax.rsqrt(jnp.mean(rows_f * rows_f, axis=-1, keepdims=True) + epsilon)
 
@@ -131,57 +138,68 @@
     piece = dot(pick, normed(0)).astype(BF)
     piece_ref[...] = piece
     x[0, 0:cap, :] = piece[0:cap]
-    both = normed(2)
-    for g in range(0, CHUNKS, 2):
-        both_ref[chunk(g), :] = dot(pick[g * step : (g + 1) * step], both).astype(BF)
-    x[2, 0:cap, :] = both_ref[0:cap, :]
     pl.semaphore_wait(barrier, n + 1)
 
-    sent = []
+    def count(r):
+        return x.at[0, pl.ds(0, r)]
+
     disp, disp2 = [None] * n, [None] * n
     for d in range(1, n):
-        disp[d] = send(piece_ref.at[slots(d)], x.at[0, slots(d)], disp_s.at[d], disp_r.at[d], (partner(d), j))
-        sent.append(disp[d])
+        to = (partner(d), j)
+        disp[d] = send(piece_ref.at[slots(d)], x.at[0, slots(d)], sent_s.at[DISPATCH], disp_r.at[d - 1], to)
         if d < n // 2:
-            disp2[d] = send(both_ref.at[slots(d)], x.at[2, slots(d)], both_s.at[d], both_r.at[d], (partner(d), j))
-            sent.append(disp2[d])
-
-    def dispatch(g):
-        for p in of(g):
+            disp2[d] = send(both_ref.at[slots(d)], x.at[2, slots(d)], sent_s.at[BOTH], disp_r.at[d - 1], to)
+
+    def dispatch(g, which=None):
+        for p in of(g) if which is None else [of(g)[which]]:
             for d in members(p):
                 if d:
                     disp[d].start()
                     if not across(g):
                         disp2[d].start()
 
-    dispatch(1)
+    def dispatched(d):
+        rows_in = cap if d >= n // 2 else 2 * cap
+        send(count(rows_in), count(rows_in), sent_s.at[DISPATCH], disp_r.at[d - 1], (partner(d), j)).wait_recv()
+
+    dispatch(1, 0)
+    both = normed(2)
+    for g in range(0, CHUNKS, 2):
+        both_ref[chunk(g), :] = dot(pick[g * step : (g + 1) * step], both).astype(BF)
+    x[2, 0:cap, :] = both_ref[0:cap, :]
     dispatch(0)
-
-    y_c, c0_c, c2_c = [], [], []
+    dispatch(1, 1)
+
+    pieces_across = [p for p in range(PIECES) if across(p * CHUNKS // PIECES)]
+    y_c, c0_c, c2_c = [None] * PIECES, [], []
     for p in range(PIECES):
-        r = bit(p)
-        y_c.append(send(x.at[0, r], x.at[2, r], y_s.at[p], y_r.at[p], (i, j2)))
-        c0_c.append(send(x.at[0, r], x.at[1, r], c_s.at[p, 0], c_r.at[p, 0], (i, j1)))
-        c2_c.append(send(x.at[2, r], x.at[3, r], c_s.at[p, 1], c_r.at[p, 1], (i, j1)))
-        sent += [c0_c[p], c2_c[p]]
-        if across(p * CHUNKS // PIECES):
-            sent.append(y_c[p])
+        r, g = bit(p), p * CHUNKS // PIECES
+        first = 3 * (g // 2) + (1 if across(g) else 0)
+        if across(g):
+            y_c[p] = send(
+                x.at[0, r], x.at[2, r], sent_s.at[ACROSS], y_r.at[pieces_across.index(p)], (i, j2)
+            )
+        c0_c.append(send(x.at[0, r], x.at[1, r], sent_s.at[CORE], c_r.at[first], (i, j1)))
+        c2_c.append(send(x.at[2, r], x.at[3, r], sent_s.at[CORE], c_r.at[first + across(g)], (i, j1)))
+
+    def arrive(g, which=0):
+        first = 3 * (g // 2) + (1 + which if across(g) else 0)
+        rows_in = step if across(g) else 2 * step
+        send(count(rows_in), count(rows_in), sent_s.at[CORE], c_r.at[first], (i, j1)).wait_recv()
 
     def forward(g, which=None):
         for p in of(g) if which is None else [of(g)[which]]:
             for d in members(p):
                 if d:
-                    disp[d].wait_recv()
-                    if not across(g):
-                        disp2[d].wait_recv()
+                    dispatched(d)
             if across(g):
                 y_c[p].start()
             else:
                 c2_c[p].start()
             c0_c[p].start()
 
-    def relay(g):
-        for p in of(g):
+    def relay(g, which=None):
+        for p in of(g) if which is None else [of(g)[which]]:
             y_c[p].wait_recv()
             c2_c[p].start()
 
@@ -192,8 +210,9 @@
         lax.broadcasted_iota(jnp.int32, (length, length), 0)
         <= lax.broadcasted_iota(jnp.int32, (length, length), 1), 1.0, 0.0
     )
-    for c in loads[3:10]:
+    for c in small_loads[3:]:
         c.wait()
+    pltpu.make_async_copy(kvqg, kvqg, w_sem.at[6]).wait()
     level = lax.dot_general(
         ld_ref[...], upper, (((1,), (0,)), ((), ())),
         precision=lax.Precision.HIGHEST, preferred_element_type=F32,
@@ -210,9 +229,11 @@
     enter[...] = jnp.zeros_like(enter)
     st_c, tot_c = [], []
     for r in range(rounds):
-        later = (lax.rem(i + (1 << r), n), j)
+        later = (lax.rem(i + (1 << r), n) if r else partner(1), j)
         st_c.append(send(st.at[r], st_in.at[r], st_s.at[r], st_r.at[r], later))
         tot_c.append(send(tot.at[r], tot_in.at[r], tot_s.at[r], tot_r.at[r], later))
+
+    second = lax.rem(i, 2) == 1
 
     def pass_on(r):
         @pl.when(i + (1 << r) < n)
@@ -226,6 +247,16 @@
         return jnp.concatenate(
             [jnp.broadcast_to(jnp.exp(totals[h : h + 1, :]), (dim, dim)) for h in range(heads)], axis=0
         )
+
+    def pair():
+        st_c[0].wait_recv()
+        tot_c[0].wait_recv()
+        own, arrived = window[...], st_in[0].astype(F32)
+        late = spread_rows(jnp.where(second, tot[0], tot_in[0]))
+        window[...] = late * jnp.where(second, arrived, own) + jnp.where(second, own, arrived)
+        st[1] = window[...].astype(BF)
+        tot[1] = tot[0] + tot_in[0]
+        pass_on(1)
 
     def absorb(r):
         @pl.when(i >= 1 << r)
@@ -247,7 +278,8 @@
             tot[r + 1] = tot[r] + tot_in[r]
             pass_on(r + 1)
 
-    pass_on(0)
+    st_c[0].start()
+    tot_c[0].start()
     dispatch(2)
     dispatch(3)
 
@@ -260,13 +292,15 @@
     def stripe(m):
         return pl.ds(pl.multiple_of(places[m] * quarter, quarter), quarter)
 
-    mix_a = send(mx.at[stripe(1)], mr1.at[0], mix_s.at[0], mix_r.at[0], (i, j1))
-    mix_b = send(mx.at[stripe(3)], mr1.at[1], mix_s.at[1], mix_r.at[1], (i, j1))
-    mix_c = send(ms, mr2, mix_s.at[2], mix_r.at[2], (i, j2))
-    sent += [mix_a, mix_b, mix_c]
+    mix_a = send(mx.at[stripe(1)], mr1.at[0], sent_s.at[MIX], mix_r.at[0], (i, j1))
+    mix_b = send(mx.at[stripe(3)], mr1.at[1], sent_s.at[MIX], mix_r.at[1], (i, j1))
+    mix_c = send(ms, mr2, sent_s.at[MIX], mix_r.at[2], (i, j2))
 
     def retention():
-        entering = enter[...].astype(BF)
+        entering = enter[...]
+        entering = jnp.where(
+            second, spread_rows(tot_in[0]) * entering + st_in[0].astype(F32), entering
+        ).astype(BF)
         for h in range(heads):
             c = slice(h * dim, (h + 1) * dim)
             queries = (q_ref[:, c].astype(F32) * jnp.exp(cum[h])).astype(BF)
@@ -285,37 +319,35 @@
     for g in range(CHUNKS):
         r = chunk(g)
         red.append((
-            send(part.at[1, r], near.at[0, r], red_s.at[g, 0], red_r.at[g, 0], (i, j1)),
-            send(part.at[3, r], near.at[1, r], red_s.at[g, 1], red_r.at[g, 1], (i, j1)),
+            send(part.at[1, r], near.at[0, r], sent_s.at[HALVES], red_r.at[g, 0], (i, j1)),
+            send(part.at[3, r], near.at[1, r], sent_s.at[HALVES], red_r.at[g, 1], (i, j1)),
         ))
-        sent += list(red[-1])
-    for p in range(PIECES):
-        r = bit(p)
-        red_y.append(send(half.at[r], far.at[r], redy_s.at[p], redy_r.at[p], (i, j2)))
-    sent += red_y
-
-    def experts(g, between=None, after=None):
-        r = chunk(g)
-        gate, up = 0.0, 0.0
-        for m in (0, 2, 1, 3):
-            if m == 1:
-                if between is not None:
-                    between()
-                for p in of(g):
-                    c0_c[p].wait_recv()
-                    c2_c[p].wait_recv()
-            gate = gate + dot(x[m, r, :], wg[block(m), :])
-            up = up + dot(x[m, r, :], wu[block(m), :])
-        hidden = (jax.nn.silu(gate) * up).astype(BF)
-        if after is not None:
-            after()
+        for k, p in enumerate(of(g)):
+            at = 3 * (g // 2) + (1 + k if across(g) else 0)
+            red_y.append(send(half.at[bit(p)], far.at[bit(p)], sent_s.at[SUMS], redy_r.at[at], (i, j2)))
+
+    def summed(p):
+        g = p * CHUNKS // PIECES
+        if across(g):
+            red_y[p].wait_recv()
+        elif p == of(g)[0]:
+            send(count(step), count(step), sent_s.at[SUMS], redy_r.at[3 * (g // 2)], (i, j2)).wait_recv()
+
+    def gate_up(g, ms, sums=(0.0, 0.0)):
+        gate, up = sums
+        for m in ms:
+            gate = gate + dot(x[m, chunk(g), :], wg[block(m), :])
+            up = up + dot(x[m, chunk(g), :], wu[block(m), :])
+        return gate, up
+
+    def down(g, sums):
+        hidden = (jax.nn.silu(sums[0]) * sums[1]).astype(BF)
         for m in (3, 1, 2, 0):
-            part[m, r, :] = dot(hidden, wd[:, block(m)]).astype(BF)
+            part[m, chunk(g), :] = dot(hidden, wd[:, block(m)]).astype(BF)
             if m == 3:
                 red[g][1].start()
             if m == 1:
                 red[g][0].start()
-        cross(g)
 
     def cross(g):
         red[g][1].wait_recv()
@@ -324,17 +356,21 @@
             half[r, :] = (part[2, r, :].astype(F32) + near[1, r, :].astype(F32)).astype(BF)
             red_y[p].start()
 
+    groups = [members(0) + members(1), members(4) + members(5), members(2) + members(3), members(6), members(7)]
     ret = [None] * n
-    for d in range(1, n):
-        ret[d] = send(done.at[slots(d)], back.at[slots(d)], ret_s.at[d], ret_r.at[d], (partner(d), j))
-        sent.append(ret[d])
+    for k, ds in enumerate(groups):
+        for d in ds:
+            if d:
+                ret[d] = send(
+                    done.at[slots(d)], back.at[slots(d)], sent_s.at[HOME], ret_r.at[k], (partner(d), j)
+                )
 
     def home(g, which=None):
         if not which:
             red[g][0].wait_recv()
         for p in of(g) if which is None else [of(g)[which]]:
             r = bit(p)
-            red_y[p].wait_recv()
+            summed(p)
             done[r, :] = (
                 part[0, r, :].astype(F32) + near[0, r, :].astype(F32) + far[r, :].astype(F32)
             ).astype(BF)
@@ -344,52 +380,83 @@
                 else:
                     back[0:cap, :] = done[0:cap, :]
 
+    forward(1, 0)
     forward(0)
-    for c in loads[10:]:
+    for c in weight_loads:
         c.wait()
-    experts(0, after=lambda: forward(1))
-    absorb(0)
+    sums = gate_up(0, (0, 2))
+    forward(1, 1)
+    arrive(0)
+    down(0, gate_up(0, (1, 3), sums))
+    sums = gate_up(1, (0,))
+    cross(0)
+    pair()
+    arrive(1)
+    sums = gate_up(1, (1,), sums)
     comb = sum(jnp.where(slot == target[t], rw_ref[t : t + 1, :], 0.0) for t in range(top)).T
     hi = comb.astype(BF)
     hi_ref[...] = hi
     lo_ref[...] = (comb - hi.astype(F32)).astype(BF)
+    relay(1)
     forward(2)
-    relay(1)
+    sums = gate_up(1, (2,), sums)
     forward(3, 0)
-    experts(1, after=lambda: forward(3, 1))
+    arrive(1, 1)
+    down(1, gate_up(1, (3,), sums))
+    forward(3, 1)
+    sums = gate_up(2, (0, 2))
+    cross(1)
     for r in range(1, rounds - 1):
         absorb(r)
-    experts(2)
+    arrive(2)
+    sums = gate_up(2, (1, 3), sums)
+    relay(3, 0)
+    down(2, sums)
+    arrive(3)
+    sums = gate_up(3, (0,))
+    relay(3, 1)
+    sums = gate_up(3, (1,), sums)
+    cross(2)
+    sums = gate_up(3, (2,), sums)
     home(0)
-    relay(3)
-    experts(3, after=lambda: home(1, 0))
+    arrive(3, 1)
+    sums = gate_up(3, (3,), sums)
+    home(1, 0)
+    down(3, sums)
     home(1, 1)
+    cross(3)
     absorb(rounds - 1)
     retention()
     home(2)
-    home(3, 0)
     mix_cross()
     mix_c.start()
+    home(3, 0)
     home(3, 1)
 
-    def gather(g):
-        for p in of(g):
-            for d in members(p):
-                if d:
-                    ret[d].wait_recv()
-        c = slice(g * step, (g + 1) * step)
+    def gather(k):
+        ds = groups[k]
+        r = (len(ds) - (0 in ds)) * cap
+        send(count(r), count(r), sent_s.at[HOME], ret_r.at[k], (i, j1)).wait_recv()
+        c = slice(position(ds[0]) * cap, position(ds[-1]) * cap + cap)
         return dot(hi_ref[:, c], back[c, :]) + dot(lo_ref[:, c], back[c, :])
 
-    blend = gather(0) + gather(2) + gather(1)
+    blend = gather(0) + gather(1) + gather(2)
     mix_a.wait_recv()
     mix_c.wait_recv()
     mixer_ref[...] = (
         mx[stripe(0), :].astype(F32) + mr1[0].astype(F32) + mr2[...].astype(F32)
     ).astype(BF)
-    expert_ref[...] = (blend + gather(3)).astype(BF)
-    for c in sent:
-        c.wait_send()
-    for r in range(rounds):
+    blend = blend + gather(3)
+    expert_ref[...] = (blend + gather(4)).astype(BF)
+    for kind, ref in (
+        (DISPATCH, count((n - 1) * cap)), (BOTH, count((n // 2 - 1) * cap)), (ACROSS, count(rows // 2)),
+        (CORE, x.at[pl.ds(0, 2)]), (HALVES, x.at[pl.ds(0, 2)]), (SUMS, count(rows)),
+        (MIX, mx.at[pl.ds(0, 3 * quarter)]), (HOME, count((n - 1) * cap)),
+    ):
+        send(ref, ref, sent_s.at[kind], ret_r.at[0], (i, j1)).wait_send()
+    st_c[0].wait_send()
+    tot_c[0].wait_send()
+    for r in range(1, rounds):
         @pl.when(i + (1 << r) < n)
         def _():
             st_c[r].wait_send()
@@ -428,8 +495,8 @@
     hbm = pl.BlockSpec(memory_space=pltpu.HBM)
     dma = pltpu.SemaphoreType.DMA
     args = (
-        moe_input, route_ids.T, moe_gain.reshape(1, full), log_decay.T, key_rows, value_rows, queries,
-        route_weights.T, out_gate, head_gain, out_weight, expert_gate[0], expert_up[0], expert_down[0],
+        moe_input, route_ids.T, moe_gain.reshape(1, full), log_decay.T, route_weights.T, head_gain,
+        key_rows, value_rows, queries, out_gate, out_weight, expert_gate[0], expert_up[0], expert_down[0],
     )
     args = [pltpu.with_memory_space_constraint(a, pltpu.HBM) for a in args]
     mixer, blended = pl.pallas_call(
@@ -440,7 +507,8 @@
         ),
         in_specs=[hbm] * len(args),
         out_specs=(vmem, vmem),
-        scratch_shapes=[pltpu.VMEM(a.shape, a.dtype) for a in args[:10]] + [
+        scratch_shapes=[pltpu.VMEM(a.shape, a.dtype) for a in args[:6]] + [
+            pltpu.VMEM((4, length, heads * dim), BF),
             pltpu.VMEM(out_weight.shape, BF),
             pltpu.VMEM((full, hidden), BF),
             pltpu.VMEM((full, hidden), BF),
@@ -464,14 +532,9 @@
             pltpu.VMEM((2, quarter, full), BF),
             pltpu.VMEM((quarter, full), BF),
             pltpu.VMEM((quarter, full), BF),
-            dma((len(args),)),
-            dma((n,)), dma((n,)), dma((n,)), dma((n,)),
+            dma((11,)), dma((8,)), dma((n - 1,)),
             dma((rounds,)), dma((rounds,)), dma((rounds,)), dma((rounds,)),
-            dma((PIECES,)), dma((PIECES,)), dma((PIECES, 2)), dma((PIECES, 2)),
-            dma((CHUNKS, 2)), dma((CHUNKS, 2)),
-            dma((PIECES,)), dma((PIECES,)),
-            dma((3,)), dma((3,)),
-            dma((n,)), dma((n,)),
+            dma((PIECES // 2,)), dma((6,)), dma((CHUNKS, 2)), dma((6,)), dma((3,)), dma((5,)),
             pltpu.VMEM((rows, width), BF),
             pltpu.VMEM((rows, width), BF),
             pltpu.VMEM((tokens, rows), BF),

time: 43.5 us -> 41.4 us (0.952)
  Pallas kernels: 42.7 us -> 40.6 us
    pallas_call x1, Pallas kernels: 41.9 us -> 39.9 us  [per_device(): pl.pallas_call(functools.partial(layer_kernel, n, cap, heads), out_shape=...]
where the time goes in v3:
time: 41.4 us; the launch traced here: 41.3 us
  Pallas kernels  40.6 us (98%)
  between operations  0.64 us (2%)
    pallas_call x1, Pallas kernels, per_device(): pl.pallas_call(functools.partial(layer_kernel, n, cap, heads), out_shape=...  39.9 us

profile of v3, /device:TPU:0, one launch (start us, length us, event | category | flops | bytes accessed | tf_op | source)
XLA Modules:
  0.0 41.3 jit_solution(8019255452977957340)
XLA Ops:
  0.6 39.9 %shard_map.149 = (bf16[64,2048]{1,0:T(8,128)(2,1)S(1)}, bf16[128,512]{1,0:T(8,128)(2,1)S(1)}) custom-call(bf16[128,2048]{1,0:T(8,128)(2,1)} %tok_hbm.1, s32[2,128]{1,0:T(2,128)} %bitcast.12, f32[1,2048]{1,0:T(1,128)} %bitcast.10, f32[2,256]{1,0:T(2,128)} %bitcast.11, f32[2,128]{1,0:T(2,128)} %bitcast.13, f32[2,128]{1,0:T(2,128)} %gain_hbm.1, ...), custom_call_target="tpu_custom_call" | custom-call | tf_op jit(solution)/shard_map/pallas_call | solution.py:502
  40.5 0.8 %shard_map.150 = (bf16[64,2048]{1,0:T(8,128)(2,1)}, bf16[128,512]{1,0:T(8,128)(2,1)}) custom-call(bf16[64,2048]{1,0:T(8,128)(2,1)S(1)} %get-tuple-element.4.mixer, bf16[128,512]{1,0:T(8,128)(2,1)S(1)} %get-tuple-element.5.blended), custom_call_target="tpu_custom_call" | custom-call | tf_op jit(solution)/shard_map/pallas_call | solution.py:547

commit v4 on v3

--- a/solution.py
+++ b/solution.py
@@ -8,8 +8,9 @@
 from jax.sharding import PartitionSpec as P
 
 epsilon = 1e-06
-CHUNKS = 4
 PIECES = 8
+GROUPS = ((0,), (2, 3), (4, 5), (6, 7), (1,))
+ACROSS_GROUPS = (1, 3)
 BF = jnp.bfloat16
 F32 = jnp.float32
 
@@ -35,7 +36,6 @@
     j3 = lax.rem(j1 + 2, 4)
     places = (j, j1, j2, j3)
     rows = n * cap
-    step = rows // CHUNKS
     small = rows // PIECES
     width = x.shape[2]
     dim = gain_ref.shape[1]
@@ -63,16 +63,22 @@
         return pl.ds(position(d) * cap, cap)
 
     def chunk(g):
-        return pl.ds(g * step, step)
+        return pl.ds(GROUPS[g][0] * small, len(GROUPS[g]) * small)
+
+    def amount(g):
+        return len(GROUPS[g]) * small
 
     def bit(p):
         return pl.ds(p * small, small)
 
     def of(g):
-        return range(g * PIECES // CHUNKS, (g + 1) * PIECES // CHUNKS)
+        return GROUPS[g]
 
     def across(g):
-        return g % 2 == 1
+        return g in ACROSS_GROUPS
+
+    def index(g, which):
+        return sum(2 if across(e) else 1 for e in range(g)) + (which if across(g) else 0)
 
     def send(src, dst, ss, rs, dev):
         return pltpu.make_async_remote_copy(
@@ -164,28 +170,29 @@
 
     dispatch(1, 0)
     both = normed(2)
-    for g in range(0, CHUNKS, 2):
-        both_ref[chunk(g), :] = dot(pick[g * step : (g + 1) * step], both).astype(BF)
+    for a in (0, rows // 2):
+        r = slice(a, a + rows // 4)
+        both_ref[r, :] = dot(pick[r], both).astype(BF)
     x[2, 0:cap, :] = both_ref[0:cap, :]
     dispatch(0)
+    dispatch(4)
     dispatch(1, 1)
 
-    pieces_across = [p for p in range(PIECES) if across(p * CHUNKS // PIECES)]
-    y_c, c0_c, c2_c = [None] * PIECES, [], []
-    for p in range(PIECES):
-        r, g = bit(p), p * CHUNKS // PIECES
-        first = 3 * (g // 2) + (1 if across(g) else 0)
-        if across(g):
-            y_c[p] = send(
-                x.at[0, r], x.at[2, r], sent_s.at[ACROSS], y_r.at[pieces_across.index(p)], (i, j2)
-            )
-        c0_c.append(send(x.at[0, r], x.at[1, r], sent_s.at[CORE], c_r.at[first], (i, j1)))
-        c2_c.append(send(x.at[2, r], x.at[3, r], sent_s.at[CORE], c_r.at[first + across(g)], (i, j1)))
+    pieces_across = [p for g in ACROSS_GROUPS for p in of(g)]
+    y_c, c0_c, c2_c = [None] * PIECES, [None] * PIECES, [None] * PIECES
+    for g in range(len(GROUPS)):
+        for p in of(g):
+            r = bit(p)
+            if across(g):
+                y_c[p] = send(
+                    x.at[0, r], x.at[2, r], sent_s.at[ACROSS], y_r.at[pieces_across.index(p)], (i, j2)
+                )
+            c0_c[p] = send(x.at[0, r], x.at[1, r], sent_s.at[CORE], c_r.at[index(g, 0)], (i, j1))
+            c2_c[p] = send(x.at[2, r], x.at[3, r], sent_s.at[CORE], c_r.at[index(g, 1)], (i, j1))
 
     def arrive(g, which=0):
-        first = 3 * (g // 2) + (1 + which if across(g) else 0)
-        rows_in = step if across(g) else 2 * step
-        send(count(rows_in), count(rows_in), sent_s.at[CORE], c_r.at[first], (i, j1)).wait_recv()
+        rows_in = amount(g) if across(g) else 2 * amount(g)
+        send(count(rows_in), count(rows_in), sent_s.at[CORE], c_r.at[index(g, which)], (i, j1)).wait_recv()
 
     def forward(g, which=None):
         for p in of(g) if which is None else [of(g)[which]]:
@@ -278,6 +285,7 @@
             tot[r + 1] = tot[r] + tot_in[r]
             pass_on(r + 1)
 
+    forward(0)
     st_c[0].start()
     tot_c[0].start()
     dispatch(2)
@@ -315,23 +323,22 @@
         mix_b.wait_recv()
         ms[...] = (mx[stripe(2), :].astype(F32) + mr1[1].astype(F32)).astype(BF)
 
-    red, red_y = [], []
-    for g in range(CHUNKS):
+    red, red_y = [], [None] * PIECES
+    for g in range(len(GROUPS)):
         r = chunk(g)
         red.append((
             send(part.at[1, r], near.at[0, r], sent_s.at[HALVES], red_r.at[g, 0], (i, j1)),
             send(part.at[3, r], near.at[1, r], sent_s.at[HALVES], red_r.at[g, 1], (i, j1)),
         ))
         for k, p in enumerate(of(g)):
-            at = 3 * (g // 2) + (1 + k if across(g) else 0)
-            red_y.append(send(half.at[bit(p)], far.at[bit(p)], sent_s.at[SUMS], redy_r.at[at], (i, j2)))
-
-    def summed(p):
-        g = p * CHUNKS // PIECES
+            red_y[p] = send(half.at[bit(p)], far.at[bit(p)], sent_s.at[SUMS], redy_r.at[index(g, k)], (i, j2))
+
+    def summed(g, k):
         if across(g):
-            red_y[p].wait_recv()
-        elif p == of(g)[0]:
-            send(count(step), count(step), sent_s.at[SUMS], redy_r.at[3 * (g // 2)], (i, j2)).wait_recv()
+            red_y[of(g)[k]].wait_recv()
+        elif k == 0:
+            r = amount(g)
+            send(count(r), count(r), sent_s.at[SUMS], redy_r.at[index(g, 0)], (i, j2)).wait_recv()
 
     def gate_up(g, ms, sums=(0.0, 0.0)):
         gate, up = sums
@@ -368,9 +375,10 @@
     def home(g, which=None):
         if not which:
             red[g][0].wait_recv()
-        for p in of(g) if which is None else [of(g)[which]]:
+        for k in range(len(of(g))) if which is None else [which]:
+            p = of(g)[k]
             r = bit(p)
-            summed(p)
+            summed(g, k)
             done[r, :] = (
                 part[0, r, :].astype(F32) + near[0, r, :].astype(F32) + far[r, :].astype(F32)
             ).astype(BF)
@@ -380,16 +388,19 @@
                 else:
                     back[0:cap, :] = done[0:cap, :]
 
-    forward(1, 0)
-    forward(0)
     for c in weight_loads:
         c.wait()
-    sums = gate_up(0, (0, 2))
+    arrive(0)
+    down(0, gate_up(0, (0, 2, 1, 3)))
+    forward(1, 0)
+    forward(4)
+    sums = gate_up(4, (0, 2))
     forward(1, 1)
-    arrive(0)
-    down(0, gate_up(0, (1, 3), sums))
+    cross(0)
+    arrive(4)
+    down(4, gate_up(4, (1, 3), sums))
     sums = gate_up(1, (0,))
-    cross(0)
+    cross(4)
     pair()
     arrive(1)
     sums = gate_up(1, (1,), sums)
@@ -398,18 +409,18 @@
     hi_ref[...] = hi
     lo_ref[...] = (comb - hi.astype(F32)).astype(BF)
     relay(1)
-    forward(2)
     sums = gate_up(1, (2,), sums)
     forward(3, 0)
     arrive(1, 1)
     down(1, gate_up(1, (3,), sums))
+    forward(2)
     forward(3, 1)
     sums = gate_up(2, (0, 2))
     cross(1)
+    arrive(2)
+    sums = gate_up(2, (1, 3), sums)
     for r in range(1, rounds - 1):
         absorb(r)
-    arrive(2)
-    sums = gate_up(2, (1, 3), sums)
     relay(3, 0)
     down(2, sums)
     arrive(3)
@@ -418,13 +429,13 @@
     sums = gate_up(3, (1,), sums)
     cross(2)
     sums = gate_up(3, (2,), sums)
+    home(1, 0)
+    arrive(3, 1)
+    down(3, gate_up(3, (3,), sums))
+    home(1, 1)
     home(0)
-    arrive(3, 1)
-    sums = gate_up(3, (3,), sums)
-    home(1, 0)
-    down(3, sums)
-    home(1, 1)
     cross(3)
+    home(4)
     absorb(rounds - 1)
     retention()
     home(2)
@@ -534,7 +545,7 @@
             pltpu.VMEM((quarter, full), BF),
             dma((11,)), dma((8,)), dma((n - 1,)),
             dma((rounds,)), dma((rounds,)), dma((rounds,)), dma((rounds,)),
-            dma((PIECES // 2,)), dma((6,)), dma((CHUNKS, 2)), dma((6,)), dma((3,)), dma((5,)),
+            dma((PIECES // 2,)), dma((7,)), dma((len(GROUPS), 2)), dma((7,)), dma((3,)), dma((5,)),
             pltpu.VMEM((rows, width), BF),
             pltpu.VMEM((rows, width), BF),
             pltpu.VMEM((tokens, rows), BF),

time: 41.4 us -> 40.7 us (0.983)
  Pallas kernels: 40.6 us -> 39.9 us
    pallas_call x1, Pallas kernels: 39.9 us -> 39.1 us  [per_device(): pl.pallas_call(functools.partial(layer_kernel, n, cap, heads), out_shape=...]
where the time goes in v4:
time: 40.7 us; the launch traced here: 40.5 us
  Pallas kernels  39.9 us (98%)
  between operations  0.64 us (2%)
    pallas_call x1, Pallas kernels, per_device(): pl.pallas_call(functools.partial(layer_kernel, n, cap, heads), out_shape=...  39.1 us

profile of v4, /device:TPU:0, one launch (start us, length us, event | category | flops | bytes accessed | tf_op | source)
XLA Modules:
  0.0 40.5 jit_solution(16263830967489242975)
XLA Ops:
  0.6 39.1 %shard_map.149 = (bf16[64,2048]{1,0:T(8,128)(2,1)S(1)}, bf16[128,512]{1,0:T(8,128)(2,1)S(1)}) custom-call(bf16[128,2048]{1,0:T(8,128)(2,1)} %tok_hbm.1, s32[2,128]{1,0:T(2,128)} %bitcast.12, f32[1,2048]{1,0:T(1,128)} %bitcast.10, f32[2,256]{1,0:T(2,128)} %bitcast.11, f32[2,128]{1,0:T(2,128)} %bitcast.13, f32[2,128]{1,0:T(2,128)} %gain_hbm.1, ...), custom_call_target="tpu_custom_call" | custom-call | tf_op jit(solution)/shard_map/pallas_call | solution.py:513
  39.8 0.8 %shard_map.150 = (bf16[64,2048]{1,0:T(8,128)(2,1)}, bf16[128,512]{1,0:T(8,128)(2,1)}) custom-call(bf16[64,2048]{1,0:T(8,128)(2,1)S(1)} %get-tuple-element.4.mixer, bf16[128,512]{1,0:T(8,128)(2,1)S(1)} %get-tuple-element.5.blended), custom_call_target="tpu_custom_call" | custom-call | tf_op jit(solution)/shard_map/pallas_call | solution.py:558

commit v5 on v4

--- a/solution.py
+++ b/solution.py
@@ -28,7 +28,7 @@
     ow, wg, wu, wd, x, part, near, half, far, done, back,
     st, st_in, tot, tot_in, window, enter, inner, ho, mx, mr1, ms, mr2,
     w_sem, sent_s, disp_r, st_s, st_r, tot_s, tot_r, y_r, c_r, red_r, redy_r, mix_r, ret_r,
-    piece_ref, both_ref, hi_ref, lo_ref,
+    piece_ref, both_ref, hi_ref, lo_ref, scaled, opened,
 ):
     i, j = lax.axis_index("ep"), lax.axis_index("tp")
     j1 = j + 1 - 2 * lax.rem(j, 2)
@@ -296,6 +296,8 @@
         scores = dot(q_ref[:, c], k_ref[:, c], (((1,), (1,)), ((), ()))) * dim ** (-0.5)
         spread = jnp.where(causal, cum[h][:, 0:1] - level[h : h + 1, :], -jnp.inf)
         inner[:, c] = dot((scores * jnp.exp(spread)).astype(BF), v_ref[:, c])
+        scaled[:, c] = (q_ref[:, c].astype(F32) * jnp.exp(cum[h])).astype(BF)
+        opened[:, c] = jax.nn.silu(g_ref[:, c].astype(F32))
 
     def stripe(m):
         return pl.ds(pl.multiple_of(places[m] * quarter, quarter), quarter)
@@ -311,10 +313,9 @@
         ).astype(BF)
         for h in range(heads):
             c = slice(h * dim, (h + 1) * dim)
-            queries = (q_ref[:, c].astype(F32) * jnp.exp(cum[h])).astype(BF)
-            kept = inner[:, c] + dot(queries, entering[h * dim : (h + 1) * dim, :])
+            kept = inner[:, c] + dot(scaled[:, c], entering[h * dim : (h + 1) * dim, :])
             unit = kept * lax.rsqrt(jnp.mean(kept * kept, axis=-1, keepdims=True) + epsilon)
-            ho[:, c] = (unit * gain_ref[h : h + 1, :] * jax.nn.silu(g_ref[:, c].astype(F32))).astype(BF)
+            ho[:, c] = (unit * gain_ref[h : h + 1, :] * opened[:, c]).astype(BF)
         mx[...] = dot(ho[...], ow[...]).astype(BF)
         mix_b.start()
         mix_a.start()
@@ -550,6 +551,8 @@
             pltpu.VMEM((rows, width), BF),
             pltpu.VMEM((tokens, rows), BF),
             pltpu.VMEM((tokens, rows), BF),
+            pltpu.VMEM((length, heads * dim), BF),
+            pltpu.VMEM((length, heads * dim), F32),
         ],
         compiler_params=pltpu.CompilerParams(
             collective_id=0, has_side_effects=True, vmem_limit_bytes=56 * 1024 * 1024

time: 40.7 us -> 40.7 us (level)
  no operation moved by 1% of the time
where the time goes in v5:
time: 40.7 us; the launch traced here: 40.5 us
  Pallas kernels  39.9 us (98%)
  between operations  0.64 us (2%)
    pallas_call x1, Pallas kernels, per_device(): pl.pallas_call(functools.partial(layer_kernel, n, cap, heads), out_shape=...  39.1 us

profile of v5, /device:TPU:0, one launch (start us, length us, event | category | flops | bytes accessed | tf_op | source)
XLA Modules:
  0.0 40.5 jit_solution(16552062745931580733)
XLA Ops:
  0.6 39.1 %shard_map.149 = (bf16[64,2048]{1,0:T(8,128)(2,1)S(1)}, bf16[128,512]{1,0:T(8,128)(2,1)S(1)}) custom-call(bf16[128,2048]{1,0:T(8,128)(2,1)} %tok_hbm.1, s32[2,128]{1,0:T(2,128)} %bitcast.12, f32[1,2048]{1,0:T(1,128)} %bitcast.10, f32[2,256]{1,0:T(2,128)} %bitcast.11, f32[2,128]{1,0:T(2,128)} %bitcast.13, f32[2,128]{1,0:T(2,128)} %gain_hbm.1, ...), custom_call_target="tpu_custom_call" | custom-call | tf_op jit(solution)/shard_map/pallas_call | solution.py:514
  39.7 0.8 %shard_map.150 = (bf16[64,2048]{1,0:T(8,128)(2,1)}, bf16[128,512]{1,0:T(8,128)(2,1)}) custom-call(bf16[64,2048]{1,0:T(8,128)(2,1)S(1)} %get-tuple-element.4.mixer, bf16[128,512]{1,0:T(8,128)(2,1)S(1)} %get-tuple-element.5.blended), custom_call_target="tpu_custom_call" | custom-call | tf_op jit(solution)/shard_map/pallas_call | solution.py:561
